TPU v7x, 32 devices: a whole 2x2x4 slice. The times are simulated.
32 devices in a mesh: sp: 4 (over z), fs: 4 (over y, x), tp: 2 (over core).
Axes of the slice: x: 2, y: 2, z: 4, core: 2. Of those that a mesh axis runs over, the one named last changes fastest.
Arguments:
- tokens: bfloat16 [4, 512, 2048], P('fs', 'sp', 'tp'), may hold values from -6 to 6
- norm_gain: float32 [2048], replicated, may hold values from 0.1 to 1.9
- conv_gate_out: bfloat16 [2048, 512], P(('sp', 'fs'), 'tp'), may hold values from -0.125 to 0.125
- conv_gate_in: bfloat16 [2048, 512], P(('sp', 'fs'), 'tp'), may hold values from -0.125 to 0.125
- conv_value: bfloat16 [2048, 512], P(('sp', 'fs'), 'tp'), may hold values from -0.125 to 0.125
- conv_taps: float32 [3, 512], P(None, 'tp'), may hold values from -3.5 to 3.5
- recv_weight: bfloat16 [2048, 512], P(('sp', 'fs'), 'tp'), may hold values from -0.125 to 0.125
- key_weight: bfloat16 [2048, 512], P(('sp', 'fs'), 'tp'), may hold values from -0.125 to 0.125
- value_weight: bfloat16 [2048, 512], P(('sp', 'fs'), 'tp'), may hold values from -0.125 to 0.125
- decay_base: float32 [512], P('tp'), may hold values from -12.5 to -3.3
- decay_down: bfloat16 [2048, 64], replicated, may hold values from -0.125 to 0.125
- decay_up: bfloat16 [64, 512], P(None, 'tp'), may hold values from -1.5 to 1.5
- decay_shift: float32 [4, 512, 8], P('fs', 'sp', 'tp'), may hold values from -0.7 to 11.5
- rate_base: float32 [512], P('tp'), may hold values from -4 to 4
- rate_down: bfloat16 [2048, 64], replicated, may hold values from -0.125 to 0.125
- rate_up: bfloat16 [64, 512], P(None, 'tp'), may hold values from -0.75 to 0.75
- head_gain: float32 [512], P('tp'), may hold values from 0.1 to 1.9
- out_conv: bfloat16 [512, 2048], P('tp', ('sp', 'fs')), may hold values from -0.1875 to 0.1875
- out_state: bfloat16 [512, 2048], P('tp', ('sp', 'fs')), may hold values from -0.1875 to 0.1875
Outputs:
- mixed_out: bfloat16 [4, 512, 2048], P('fs', ('sp', 'tp'))
All inputs are finite; a program needn't handle non-finite values.
Results may differ from a plain program's by a relative error of at most 0.015.
Values may be sent and summed in bfloat16 or wider, within the bound.
A program may use at most 64 MiB of HBM per device.

v0:
```python
from functools import partial
import math

import jax
import jax.numpy as jnp
from jax import lax
from jax.sharding import PartitionSpec as P

RMS_EPS = 1e-05
GROUP_EPS = 0.00064
UNIT_EPS = 1e-06
HIGHEST = lax.Precision.HIGHEST


def from_behind(array, axis, by):
    size = lax.axis_size(axis)
    pairs = [(i, i + by) for i in range(size) if 0 <= i + by < size]
    return lax.ppermute(array, axis, pairs)


def carried_in(array, axis, combine, identity):
    size, index = (lax.axis_size(axis), lax.axis_index(axis))
    everything = jax.tree.map(
        lambda part, kind: lax.all_gather(part.astype(kind), axis),
        array,
        (jnp.bfloat16, jnp.bfloat16),
    )
    start = jax.tree.map(
        lambda part, zero: jnp.broadcast_to(jnp.asarray(zero, part.dtype), part.shape),
        array,
        identity,
    )

    def lap(k, before):
        reached = k < index
        new = combine(
            before, jax.tree.map(lambda part, own: part[k].astype(own.dtype), everything, array)
        )
        return jax.tree.map(lambda a, b: jnp.where(reached, a, b), new, before)

    return lax.fori_loop(0, size, lap, start)


def fold_rows(normed, totals, pieces, offset):
    return tuple(
        (
            jnp.dot(normed, pieces[member], preferred_element_type=jnp.float32)
            for member in range(len(pieces))
        )
    )


def block_step(carried, inputs):
    log_dec, remove_dir, write_dir, key_rate, receive, val_rows = inputs
    cumulative = jnp.cumsum(log_dec, axis=1)
    exclusive = cumulative - log_dec
    length = log_dec.shape[1]
    where_t = lax.broadcasted_iota(jnp.int32, (length, length), 0)
    where_s = lax.broadcasted_iota(jnp.int32, (length, length), 1)
    strict = (where_t > where_s)[None, :, :, None]
    inclusive = (where_t >= where_s)[None, :, :, None]
    damp_prior = jnp.where(
        strict, jnp.exp(jnp.minimum(exclusive[:, :, None, :] - cumulative[:, None, :, :], 0.0)), 0.0
    )
    damp_now = jnp.where(
        inclusive,
        jnp.exp(jnp.minimum(cumulative[:, :, None, :] - cumulative[:, None, :, :], 0.0)),
        0.0,
    )
    link_ab = jnp.einsum("htc,htsc,hsc->hts", remove_dir, damp_prior, write_dir, precision=HIGHEST)
    link_ak = jnp.einsum("htc,htsc,hsc->hts", remove_dir, damp_prior, key_rate, precision=HIGHEST)
    from_start = jnp.einsum(
        "hrc,htc->htr", carried, remove_dir * jnp.exp(exclusive), precision=HIGHEST
    )
    rhs_terms = from_start + jnp.einsum("hts,hsr->htr", link_ak, val_rows, precision=HIGHEST)
    unit_matrix = jnp.eye(length, dtype=jnp.float32)
    projected = lax.linalg.triangular_solve(
        unit_matrix - link_ab, rhs_terms, left_side=True, lower=True, unit_diagonal=True
    )
    read_b = jnp.einsum("htc,htsc,hsc->hts", receive, damp_now, write_dir, precision=HIGHEST)
    read_k = jnp.einsum("htc,htsc,hsc->hts", receive, damp_now, key_rate, precision=HIGHEST)
    outputs = (
        jnp.einsum("hrc,htc->htr", carried, receive * jnp.exp(cumulative), precision=HIGHEST)
        + jnp.einsum("hts,hsr->htr", read_b, projected, precision=HIGHEST)
        + jnp.einsum("hts,hsr->htr", read_k, val_rows, precision=HIGHEST)
    )
    to_end = jnp.exp(cumulative[:, -1:, :] - cumulative)
    new_state = (
        carried * jnp.exp(cumulative[:, -1, :])[:, None, :]
        + jnp.einsum("hsr,hsc->hrc", projected, write_dir * to_end, precision=HIGHEST)
        + jnp.einsum("hsr,hsc->hrc", val_rows, key_rate * to_end, precision=HIGHEST)
    )
    return (new_state, outputs)


def compose(earlier, later):
    return (
        jnp.einsum("hij,hjk->hik", earlier[0], later[0], precision=HIGHEST),
        jnp.einsum("hij,hjk->hik", earlier[1], later[0], precision=HIGHEST) + later[1],
    )


def body(
    tokens,
    norm_gain,
    conv_gate_out,
    conv_gate_in,
    conv_value,
    conv_taps,
    recv_weight,
    key_weight,
    value_weight,
    decay_base,
    decay_down,
    decay_up,
    decay_shift,
    rate_base,
    rate_down,
    rate_up,
    head_gain,
    out_conv,
    out_state,
):
    tok_count = tokens.shape[1]
    own_half = tokens.reshape(tok_count, tokens.shape[2])
    features = lax.all_gather(own_half, "tp", axis=1, tiled=True).astype(jnp.float32)
    normed = (
        features
        * lax.rsqrt(jnp.mean(features * features, axis=-1, keepdims=True) + RMS_EPS)
        * norm_gain
    ).astype(jnp.bfloat16)
    widths = (
        conv_gate_out.shape[1],
        conv_gate_in.shape[1],
        conv_value.shape[1],
        recv_weight.shape[1],
        key_weight.shape[1],
        value_weight.shape[1],
    )
    zeros_init = tuple(
        (jnp.zeros((tok_count, column_count), jnp.float32) for column_count in widths)
    )
    row_adder = partial(fold_rows, normed)
    local_go, local_gi, local_cv, local_rw, local_kw, local_vw = (
        lax.all_gather(conv_gate_out, "fs", axis=0, tiled=True),
        lax.all_gather(conv_gate_in, "fs", axis=0, tiled=True),
        lax.all_gather(conv_value, "fs", axis=0, tiled=True),
        lax.all_gather(recv_weight, "fs", axis=0, tiled=True),
        lax.all_gather(key_weight, "fs", axis=0, tiled=True),
        lax.all_gather(value_weight, "fs", axis=0, tiled=True),
    )
    projected_sums = row_adder(
        zeros_init,
        (
            lax.all_gather(local_go, "sp", axis=0, tiled=True),
            lax.all_gather(local_gi, "sp", axis=0, tiled=True),
            lax.all_gather(local_cv, "sp", axis=0, tiled=True),
            lax.all_gather(local_rw, "sp", axis=0, tiled=True),
            lax.all_gather(local_kw, "sp", axis=0, tiled=True),
            lax.all_gather(local_vw, "sp", axis=0, tiled=True),
        ),
        jnp.int32(0),
    )
    gate_out, gate_in, conv_in, recv_raw, keys_raw, vals_raw = tuple(
        (member.astype(jnp.bfloat16) for member in projected_sums)
    )
    mixed_in = gate_in.astype(jnp.float32) * conv_in.astype(jnp.float32)
    edge_rows = from_behind(mixed_in[-2:], "sp", 1)
    padded = jnp.concatenate([edge_rows, mixed_in], axis=0)
    convolved = (
        padded[0:tok_count] * conv_taps[0]
        + padded[1 : tok_count + 1] * conv_taps[1]
        + padded[2:] * conv_taps[2]
    )
    conv_out = (gate_out.astype(jnp.float32) * convolved).astype(jnp.bfloat16)
    heads_here = decay_shift.shape[2]
    head_size = recv_raw.shape[1] // heads_here
    shaped = (tok_count, heads_here, head_size)
    decay_low = jnp.tanh(jnp.dot(normed, decay_down, preferred_element_type=jnp.float32)).astype(
        jnp.bfloat16
    )
    rate_low = jnp.dot(normed, rate_down, preferred_element_type=jnp.float32).astype(jnp.bfloat16)
    decay_pre = decay_base + jnp.dot(decay_low, decay_up, preferred_element_type=jnp.float32)
    log_base = -jax.nn.softplus(-decay_pre) - 0.5
    log_decay = -jnp.exp(log_base.reshape(shaped) + decay_shift.reshape(tok_count, heads_here, 1))
    learn_rate = jax.nn.sigmoid(
        rate_base + jnp.dot(rate_low, rate_up, preferred_element_type=jnp.float32)
    ).reshape(shaped)
    keys_float = keys_raw.astype(jnp.float32).reshape(shaped)
    unit_keys = keys_float * lax.rsqrt(
        jnp.sum(keys_float * keys_float, axis=-1, keepdims=True) + UNIT_EPS
    )
    values_float = vals_raw.astype(jnp.float32).reshape(shaped)
    recv_float = recv_raw.astype(jnp.float32).reshape(shaped)
    block_len = math.gcd(tok_count, 32)
    blocks = tok_count // block_len

    def to_blocks(field):
        return field.reshape(blocks, block_len, heads_here, field.shape[2]).transpose(0, 2, 1, 3)

    val_rows = jnp.concatenate([values_float, jnp.zeros_like(values_float)], axis=2)
    basis = jnp.broadcast_to(
        jnp.eye(head_size, dtype=jnp.float32), (heads_here, head_size, head_size)
    )
    empty_rows = jnp.zeros((heads_here, head_size, head_size), jnp.float32)
    start_rows = jnp.concatenate([empty_rows, basis], axis=1)
    end_rows, outputs = lax.scan(
        block_step,
        start_rows,
        (
            to_blocks(log_decay),
            to_blocks(-unit_keys),
            to_blocks(unit_keys * learn_rate),
            to_blocks(keys_float * learn_rate),
            to_blocks(recv_float),
            to_blocks(val_rows),
        ),
    )
    offset_part = end_rows[:, :head_size, :]
    transit = end_rows[:, head_size:, :]
    prefix = carried_in((transit, offset_part), "sp", compose, (basis, empty_rows))
    entering = prefix[1]
    direct = outputs[..., :head_size]
    through = outputs[..., head_size:]
    state_read = direct + jnp.einsum("hji,nhti->nhtj", entering, through, precision=HIGHEST)
    state_read = state_read.transpose(0, 2, 1, 3).reshape(shaped)
    centre = jnp.mean(state_read, axis=-1, keepdims=True)
    centred = state_read - centre
    variance = jnp.mean(centred * centred, axis=-1, keepdims=True)
    state_out = (
        (centred * lax.rsqrt(variance + GROUP_EPS)).reshape(tok_count, heads_here * head_size)
        * head_gain
    ).astype(jnp.bfloat16)
    local_oc, local_os = (
        lax.all_gather(out_conv, "fs", axis=1, tiled=True),
        lax.all_gather(out_state, "fs", axis=1, tiled=True),
    )
    conv_cols, state_cols = (
        lax.all_gather(local_oc, "sp", axis=1, tiled=True),
        lax.all_gather(local_os, "sp", axis=1, tiled=True),
    )
    tp_count = lax.axis_size("tp")
    own_rows = tok_count // tp_count
    merged = lax.psum_scatter(
        (
            jnp.dot(conv_out, conv_cols, preferred_element_type=jnp.float32)
            + jnp.dot(state_out, state_cols, preferred_element_type=jnp.float32)
        ).astype(jnp.bfloat16),
        "tp",
        scatter_dimension=0,
        tiled=True,
    ).astype(jnp.float32)
    return merged.astype(jnp.bfloat16).reshape(1, own_rows, merged.shape[1])


def solution(mesh):
    placed = (
        P("fs", "sp", "tp"),
        P(),
        P(("sp", "fs"), "tp"),
        P(("sp", "fs"), "tp"),
        P(("sp", "fs"), "tp"),
        P(None, "tp"),
        P(("sp", "fs"), "tp"),
        P(("sp", "fs"), "tp"),
        P(("sp", "fs"), "tp"),
        P("tp"),
        P(),
        P(None, "tp"),
        P("fs", "sp", "tp"),
        P("tp"),
        P(),
        P(None, "tp"),
        P("tp"),
        P("tp", ("sp", "fs")),
        P("tp", ("sp", "fs")),
    )
    return jax.shard_map(
        body, mesh=mesh, in_specs=placed, out_specs=P("fs", ("sp", "tp"), None), check_vma=False
    )
```

profile of v0, /device:TPU:11, one launch (start us, length us, event | category | flops | bytes accessed | tf_op | source)
XLA Modules:
  0.0 277.7 jit_solution(4372514369484368257)
XLA Ops:
  6.5 8.0 %all_gather.72 = bf16[512,256]{1,0:T(8,128)(2,1)} all-gather(bf16[128,256]{1,0:T(8,128)(2,1)} %param.30), channel_id=1, replica_groups=mesh['sp'=4,'fs'=4,'tp'=2] {'fs'}, dimensions={0}, use_global_device_ids=true | all-gather | bytes 327680 | tf_op jit(solution)/shard_map/all_gather | solution.py:149
  14.6 7.8 %all_gather.76 = bf16[512,256]{1,0:T(8,128)(2,1)} all-gather(bf16[128,256]{1,0:T(8,128)(2,1)} %param.29), channel_id=1, replica_groups=mesh['sp'=4,'fs'=4,'tp'=2] {'fs'}, dimensions={0}, use_global_device_ids=true | all-gather | bytes 327680 | tf_op jit(solution)/shard_map/all_gather | solution.py:148
  22.5 8.4 %all_gather.74 = bf16[512,256]{1,0:T(8,128)(2,1)} all-gather(bf16[128,256]{1,0:T(8,128)(2,1)S(1)} %copy-done.2), channel_id=1, replica_groups=mesh['sp'=4,'fs'=4,'tp'=2] {'fs'}, dimensions={0}, use_global_device_ids=true | all-gather | bytes 327680 | tf_op jit(solution)/shard_map/all_gather | solution.py:150
  31.0 7.8 %all_gather.66 = bf16[512,256]{1,0:T(8,128)(2,1)} all-gather(bf16[128,256]{1,0:T(8,128)(2,1)S(1)} %copy-done.3), channel_id=1, replica_groups=mesh['sp'=4,'fs'=4,'tp'=2] {'fs'}, dimensions={0}, use_global_device_ids=true | all-gather | bytes 327680 | tf_op jit(solution)/shard_map/all_gather | solution.py:146
  38.9 7.6 %all_gather.68 = bf16[512,256]{1,0:T(8,128)(2,1)} all-gather(bf16[128,256]{1,0:T(8,128)(2,1)S(1)} %copy-done.4), channel_id=1, replica_groups=mesh['sp'=4,'fs'=4,'tp'=2] {'fs'}, dimensions={0}, use_global_device_ids=true | all-gather | bytes 327680 | tf_op jit(solution)/shard_map/all_gather | solution.py:147
  46.6 7.9 %all_gather.64 = bf16[512,256]{1,0:T(8,128)(2,1)} all-gather(bf16[128,256]{1,0:T(8,128)(2,1)S(1)} %copy-done.5), channel_id=1, replica_groups=mesh['sp'=4,'fs'=4,'tp'=2] {'fs'}, dimensions={0}, use_global_device_ids=true | all-gather | bytes 327680 | tf_op jit(solution)/shard_map/all_gather | solution.py:145
  54.5 7.7 %all_gather.70 = bf16[256,512]{1,0:T(8,128)(2,1)} all-gather(bf16[256,128]{1,0:T(8,128)(2,1)S(1)} %copy-done.6), channel_id=1, replica_groups=mesh['sp'=4,'fs'=4,'tp'=2] {'fs'}, dimensions={1}, use_global_device_ids=true | all-gather | bytes 327680 | tf_op jit(solution)/shard_map/all_gather | solution.py:235
  62.3 7.9 %all_gather.82 = bf16[256,512]{1,0:T(8,128)(2,1)} all-gather(bf16[256,128]{1,0:T(8,128)(2,1)S(1)} %copy-done.7), channel_id=1, replica_groups=mesh['sp'=4,'fs'=4,'tp'=2] {'fs'}, dimensions={1}, use_global_device_ids=true | all-gather | bytes 327680 | tf_op jit(solution)/shard_map/all_gather | solution.py:236
  70.3 14.6 %all-gather = bf16[1,128,2048]{2,1,0:T(8,128)(2,1)S(1)} all-gather(bf16[1,128,1024]{2,1,0:T(8,128)(2,1)S(1)} %copy-done.1), channel_id=2, replica_groups=mesh['sp'=4,'fs'=4,'tp'=2] {'tp'}, dimensions={2}, use_global_device_ids=true | all-gather | bytes 786432 | tf_op jit(solution)/shard_map/all_gather | solution.py:126
  85.2 0.6 fusion.74
  86.1 0.7 fusion.97
  87.2 1.6 fusion.122
  89.2 1.6 fusion.76
  90.9 11.7 %all-gather.22.cloned.1.call-done = bf16[2048,256]{1,0:T(8,128)(2,1)} async-done(((bf16[512,256]{1,0:T(8,128)(2,1)}), bf16[2048,256]{1,0:T(8,128)(2,1)}) %all-gather.22.cloned.1.call-update) | async-done | bytes 1048592 | tf_op jit(solution)/shard_map/all_gather | solution.py:160
  102.6 1.6 convolution_convert_fusion.1
  104.8 111.5 %while.26 = (s32[]{:T(128)}, f32[4,128,64]{1,2,0:T(8,128)S(1)}, f32[4,4,32,128]{3,2,0,1:T(8,128)S(1)}, f32[4,4,32,64]{3,2,1,0:T(8,128)S(1)}, f32[4,4,32,64]{3,2,...) while((s32[]{:T(128)}, f32[4,128,64]{1,2,0:T(8,128)S(1)}, ...), condition=%wide.region_4.5_spmd, body=%wide.region_2.4_spmd.sunk | while | flops 92752928 | bytes 3343749 | solution.py:207
  105.2 3.8 %fusion.210 = f32[4,32,1,32]{3,2,1,0:T(1,128)S(1)} fusion(f32[4,32,64,1]{2,3,1,0:T(1,128)S(1)} %bitcast.246, f32[4,32,64]{2,1,0:T(8,128)S(1)} %get-tuple-element.332, f32[4,32,64]{2,1,0:T(8,128)S(1)} %reduce_window_sum.12, f32[4,32,64]{2,1,0:T(8,128)S(1)} %fusion.207, pred[32,32]{1,0:T(8,128)(4,1)S(1)} %iota_compare_fusion.9), kind=kOutput, calls=%fused_computation.6.clone.1 | convolution fusion | flops 4194304 | bytes 148480 | tf_op jit(solution)/shard_map/while/body/eval_jaxpr/htc,htsc,hsc->hts/dot_general | solution.py:70
  109.1 9.8 %custom-call.6 = f32[4,1,32,32]{2,3,1,0:T(8,128)S(1)} custom-call(f32[4,1,32,32]{3,2,1,0:T(8,128)S(1)} %add_bitcast_fusion.2), custom_call_target="InvertDiagBlocksLowerTriangular" | custom-call | tf_op jit(solution)/shard_map/while/body/eval_jaxpr/triangular_solve | solution.py:77
  119.0 3.8 %fusion.209 = f32[4,32,1,32]{3,2,1,0:T(1,128)S(1)} fusion(f32[4,32,64,1]{2,3,1,0:T(1,128)S(1)} %bitcast.247, f32[4,32,64]{2,1,0:T(8,128)S(1)} %get-tuple-element.331, f32[4,32,64]{2,1,0:T(8,128)S(1)} %reduce_window_sum.12, f32[4,32,64]{2,1,0:T(8,128)S(1)} %fusion.207, pred[32,32]{1,0:T(8,128)(4,1)S(1)} %iota_compare_fusion.9), kind=kOutput, calls=%fused_computation.4.clone.1 | convolution fusion | flops 4194304 | bytes 148480 | tf_op jit(solution)/shard_map/while/body/eval_jaxpr/htc,htsc,hsc->hts/dot_general | solution.py:71
  123.3 0.3 fusion.212
  123.6 3.8 %fusion.215 = f32[4,32,1,32]{3,2,1,0:T(1,128)S(1)} fusion(f32[4,32,64,1]{2,3,1,0:T(1,128)S(1)} %bitcast.244, f32[4,32,64]{2,1,0:T(8,128)S(1)} %reduce_window_sum.12, f32[4,32,64]{2,1,0:T(8,128)S(1)} %get-tuple-element.332, pred[32,32]{1,0:T(8,128)(4,1)S(1)} %iota_compare_fusion.11), kind=kOutput, calls=%fused_computation.2.clone.1 | convolution fusion | flops 4194304 | bytes 115712 | tf_op jit(solution)/shard_map/while/body/eval_jaxpr/htc,htsc,hsc->hts/dot_general | solution.py:80
  127.9 3.8 %fusion.216 = f32[4,32,1,32]{3,2,1,0:T(1,128)S(1)} fusion(f32[4,32,64,1]{2,3,1,0:T(1,128)S(1)} %bitcast.245, f32[4,32,64]{2,1,0:T(8,128)S(1)} %reduce_window_sum.12, f32[4,32,64]{2,1,0:T(8,128)S(1)} %get-tuple-element.331, pred[32,32]{1,0:T(8,128)(4,1)S(1)} %iota_compare_fusion.11), kind=kOutput, calls=%fused_computation.clone.1 | convolution fusion | flops 4194304 | bytes 115712 | tf_op jit(solution)/shard_map/while/body/eval_jaxpr/htc,htsc,hsc->hts/dot_general | solution.py:81
  131.9 0.4 convolution_add_fusion.13
  132.3 0.4 convolution_add_fusion.14
  132.9 3.8 %fusion.210 = f32[4,32,1,32]{3,2,1,0:T(1,128)S(1)} fusion(f32[4,32,64,1]{2,3,1,0:T(1,128)S(1)} %bitcast.246, f32[4,32,64]{2,1,0:T(8,128)S(1)} %get-tuple-element.332, f32[4,32,64]{2,1,0:T(8,128)S(1)} %reduce_window_sum.12, f32[4,32,64]{2,1,0:T(8,128)S(1)} %fusion.207, pred[32,32]{1,0:T(8,128)(4,1)S(1)} %iota_compare_fusion.9), kind=kOutput, calls=%fused_computation.6.clone.1 | convolution fusion | flops 4194304 | bytes 148480 | tf_op jit(solution)/shard_map/while/body/eval_jaxpr/htc,htsc,hsc->hts/dot_general | solution.py:70
  136.9 9.8 %custom-call.6 = f32[4,1,32,32]{2,3,1,0:T(8,128)S(1)} custom-call(f32[4,1,32,32]{3,2,1,0:T(8,128)S(1)} %add_bitcast_fusion.2), custom_call_target="InvertDiagBlocksLowerTriangular" | custom-call | tf_op jit(solution)/shard_map/while/body/eval_jaxpr/triangular_solve | solution.py:77
  146.7 3.8 %fusion.209 = f32[4,32,1,32]{3,2,1,0:T(1,128)S(1)} fusion(f32[4,32,64,1]{2,3,1,0:T(1,128)S(1)} %bitcast.247, f32[4,32,64]{2,1,0:T(8,128)S(1)} %get-tuple-element.331, f32[4,32,64]{2,1,0:T(8,128)S(1)} %reduce_window_sum.12, f32[4,32,64]{2,1,0:T(8,128)S(1)} %fusion.207, pred[32,32]{1,0:T(8,128)(4,1)S(1)} %iota_compare_fusion.9), kind=kOutput, calls=%fused_computation.4.clone.1 | convolution fusion | flops 4194304 | bytes 148480 | tf_op jit(solution)/shard_map/while/body/eval_jaxpr/htc,htsc,hsc->hts/dot_general | solution.py:71
  151.0 0.3 fusion.212
  151.3 3.8 %fusion.215 = f32[4,32,1,32]{3,2,1,0:T(1,128)S(1)} fusion(f32[4,32,64,1]{2,3,1,0:T(1,128)S(1)} %bitcast.244, f32[4,32,64]{2,1,0:T(8,128)S(1)} %reduce_window_sum.12, f32[4,32,64]{2,1,0:T(8,128)S(1)} %get-tuple-element.332, pred[32,32]{1,0:T(8,128)(4,1)S(1)} %iota_compare_fusion.11), kind=kOutput, calls=%fused_computation.2.clone.1 | convolution fusion | flops 4194304 | bytes 115712 | tf_op jit(solution)/shard_map/while/body/eval_jaxpr/htc,htsc,hsc->hts/dot_general | solution.py:80
  155.6 3.8 %fusion.216 = f32[4,32,1,32]{3,2,1,0:T(1,128)S(1)} fusion(f32[4,32,64,1]{2,3,1,0:T(1,128)S(1)} %bitcast.245, f32[4,32,64]{2,1,0:T(8,128)S(1)} %reduce_window_sum.12, f32[4,32,64]{2,1,0:T(8,128)S(1)} %get-tuple-element.331, pred[32,32]{1,0:T(8,128)(4,1)S(1)} %iota_compare_fusion.11), kind=kOutput, calls=%fused_computation.clone.1 | convolution fusion | flops 4194304 | bytes 115712 | tf_op jit(solution)/shard_map/while/body/eval_jaxpr/htc,htsc,hsc->hts/dot_general | solution.py:81
  159.7 0.4 convolution_add_fusion.13
  160.1 0.4 convolution_add_fusion.14
  160.7 3.8 %fusion.210 = f32[4,32,1,32]{3,2,1,0:T(1,128)S(1)} fusion(f32[4,32,64,1]{2,3,1,0:T(1,128)S(1)} %bitcast.246, f32[4,32,64]{2,1,0:T(8,128)S(1)} %get-tuple-element.332, f32[4,32,64]{2,1,0:T(8,128)S(1)} %reduce_window_sum.12, f32[4,32,64]{2,1,0:T(8,128)S(1)} %fusion.207, pred[32,32]{1,0:T(8,128)(4,1)S(1)} %iota_compare_fusion.9), kind=kOutput, calls=%fused_computation.6.clone.1 | convolution fusion | flops 4194304 | bytes 148480 | tf_op jit(solution)/shard_map/while/body/eval_jaxpr/htc,htsc,hsc->hts/dot_general | solution.py:70
  164.7 9.8 %custom-call.6 = f32[4,1,32,32]{2,3,1,0:T(8,128)S(1)} custom-call(f32[4,1,32,32]{3,2,1,0:T(8,128)S(1)} %add_bitcast_fusion.2), custom_call_target="InvertDiagBlocksLowerTriangular" | custom-call | tf_op jit(solution)/shard_map/while/body/eval_jaxpr/triangular_solve | solution.py:77
  174.5 3.8 %fusion.209 = f32[4,32,1,32]{3,2,1,0:T(1,128)S(1)} fusion(f32[4,32,64,1]{2,3,1,0:T(1,128)S(1)} %bitcast.247, f32[4,32,64]{2,1,0:T(8,128)S(1)} %get-tuple-element.331, f32[4,32,64]{2,1,0:T(8,128)S(1)} %reduce_window_sum.12, f32[4,32,64]{2,1,0:T(8,128)S(1)} %fusion.207, pred[32,32]{1,0:T(8,128)(4,1)S(1)} %iota_compare_fusion.9), kind=kOutput, calls=%fused_computation.4.clone.1 | convolution fusion | flops 4194304 | bytes 148480 | tf_op jit(solution)/shard_map/while/body/eval_jaxpr/htc,htsc,hsc->hts/dot_general | solution.py:71
  178.8 0.3 fusion.212
  179.1 3.8 %fusion.215 = f32[4,32,1,32]{3,2,1,0:T(1,128)S(1)} fusion(f32[4,32,64,1]{2,3,1,0:T(1,128)S(1)} %bitcast.244, f32[4,32,64]{2,1,0:T(8,128)S(1)} %reduce_window_sum.12, f32[4,32,64]{2,1,0:T(8,128)S(1)} %get-tuple-element.332, pred[32,32]{1,0:T(8,128)(4,1)S(1)} %iota_compare_fusion.11), kind=kOutput, calls=%fused_computation.2.clone.1 | convolution fusion | flops 4194304 | bytes 115712 | tf_op jit(solution)/shard_map/while/body/eval_jaxpr/htc,htsc,hsc->hts/dot_general | solution.py:80
  183.4 3.8 %fusion.216 = f32[4,32,1,32]{3,2,1,0:T(1,128)S(1)} fusion(f32[4,32,64,1]{2,3,1,0:T(1,128)S(1)} %bitcast.245, f32[4,32,64]{2,1,0:T(8,128)S(1)} %reduce_window_sum.12, f32[4,32,64]{2,1,0:T(8,128)S(1)} %get-tuple-element.331, pred[32,32]{1,0:T(8,128)(4,1)S(1)} %iota_compare_fusion.11), kind=kOutput, calls=%fused_computation.clone.1 | convolution fusion | flops 4194304 | bytes 115712 | tf_op jit(solution)/shard_map/while/body/eval_jaxpr/htc,htsc,hsc->hts/dot_general | solution.py:81
  187.4 0.4 convolution_add_fusion.13
  187.9 0.4 convolution_add_fusion.14
  188.5 3.8 %fusion.210 = f32[4,32,1,32]{3,2,1,0:T(1,128)S(1)} fusion(f32[4,32,64,1]{2,3,1,0:T(1,128)S(1)} %bitcast.246, f32[4,32,64]{2,1,0:T(8,128)S(1)} %get-tuple-element.332, f32[4,32,64]{2,1,0:T(8,128)S(1)} %reduce_window_sum.12, f32[4,32,64]{2,1,0:T(8,128)S(1)} %fusion.207, pred[32,32]{1,0:T(8,128)(4,1)S(1)} %iota_compare_fusion.9), kind=kOutput, calls=%fused_computation.6.clone.1 | convolution fusion | flops 4194304 | bytes 148480 | tf_op jit(solution)/shard_map/while/body/eval_jaxpr/htc,htsc,hsc->hts/dot_general | solution.py:70
  192.4 9.8 %custom-call.6 = f32[4,1,32,32]{2,3,1,0:T(8,128)S(1)} custom-call(f32[4,1,32,32]{3,2,1,0:T(8,128)S(1)} %add_bitcast_fusion.2), custom_call_target="InvertDiagBlocksLowerTriangular" | custom-call | tf_op jit(solution)/shard_map/while/body/eval_jaxpr/triangular_solve | solution.py:77
  202.3 3.8 %fusion.209 = f32[4,32,1,32]{3,2,1,0:T(1,128)S(1)} fusion(f32[4,32,64,1]{2,3,1,0:T(1,128)S(1)} %bitcast.247, f32[4,32,64]{2,1,0:T(8,128)S(1)} %get-tuple-element.331, f32[4,32,64]{2,1,0:T(8,128)S(1)} %reduce_window_sum.12, f32[4,32,64]{2,1,0:T(8,128)S(1)} %fusion.207, pred[32,32]{1,0:T(8,128)(4,1)S(1)} %iota_compare_fusion.9), kind=kOutput, calls=%fused_computation.4.clone.1 | convolution fusion | flops 4194304 | bytes 148480 | tf_op jit(solution)/shard_map/while/body/eval_jaxpr/htc,htsc,hsc->hts/dot_general | solution.py:71
  206.6 0.3 fusion.212
  206.9 3.8 %fusion.215 = f32[4,32,1,32]{3,2,1,0:T(1,128)S(1)} fusion(f32[4,32,64,1]{2,3,1,0:T(1,128)S(1)} %bitcast.244, f32[4,32,64]{2,1,0:T(8,128)S(1)} %reduce_window_sum.12, f32[4,32,64]{2,1,0:T(8,128)S(1)} %get-tuple-element.332, pred[32,32]{1,0:T(8,128)(4,1)S(1)} %iota_compare_fusion.11), kind=kOutput, calls=%fused_computation.2.clone.1 | convolution fusion | flops 4194304 | bytes 115712 | tf_op jit(solution)/shard_map/while/body/eval_jaxpr/htc,htsc,hsc->hts/dot_general | solution.py:80
  211.2 3.8 %fusion.216 = f32[4,32,1,32]{3,2,1,0:T(1,128)S(1)} fusion(f32[4,32,64,1]{2,3,1,0:T(1,128)S(1)} %bitcast.245, f32[4,32,64]{2,1,0:T(8,128)S(1)} %reduce_window_sum.12, f32[4,32,64]{2,1,0:T(8,128)S(1)} %get-tuple-element.331, pred[32,32]{1,0:T(8,128)(4,1)S(1)} %iota_compare_fusion.11), kind=kOutput, calls=%fused_computation.clone.1 | convolution fusion | flops 4194304 | bytes 115712 | tf_op jit(solution)/shard_map/while/body/eval_jaxpr/htc,htsc,hsc->hts/dot_general | solution.py:81
  215.2 0.4 convolution_add_fusion.13
  215.6 0.4 convolution_add_fusion.14
  216.4 10.4 %all-gather.1 = bf16[16,64,64]{2,1,0:T(8,128)(2,1)S(1)} all-gather(bf16[4,64,64]{2,1,0:T(8,128)(2,1)S(1)} %get-tuple-element.231), channel_id=3, replica_groups=mesh['sp'=4,'fs'=4,'tp'=2] {'sp'}, dimensions={0}, use_global_device_ids=true | all-gather | bytes 163840 | tf_op jit(solution)/shard_map/all_gather | solution.py:24
  226.9 14.2 %all-gather.2 = bf16[16,64,64]{2,1,0:T(8,128)(2,1)S(1)} all-gather(bf16[4,64,64]{2,1,0:T(8,128)(2,1)S(1)} %get-tuple-element.230), channel_id=4, replica_groups=mesh['sp'=4,'fs'=4,'tp'=2] {'sp'}, dimensions={0}, use_global_device_ids=true | all-gather | bytes 163840 | tf_op jit(solution)/shard_map/all_gather | solution.py:24
  241.1 1.7 while.27
  241.2 0.3 fusion.220
  241.7 0.3 fusion.220
  242.1 0.3 fusion.220
  242.6 0.3 fusion.220
  242.9 1.6 fusion.80
  244.5 1.6 fusion.79
  246.1 2.1 collective-permute-start
  248.3 0.6 fusion.123
  248.8 0.3 multiply_reduce_fusion
  250.0 1.0 collective-permute-done
  251.0 2.4 fusion.100
  253.4 2.3 fusion.68
  255.8 15.4 %reduce-scatter.2.cloned.1.call-done = bf16[64,2048]{1,0:T(8,128)(2,1)} async-done(((bf16[128,2048]{1,0:T(8,128)(2,1)}), bf16[64,2048]{1,0:T(8,128)(2,1)}) %reduce-scatter.2.cloned.1.call-update) | async-done | bytes 262160 | tf_op jit(solution)/shard_map/reduce_scatter | solution.py:244
  (176 shorter events, 9.4 us)
Async XLA Ops:
  6.5 78.6 %copy-start = (bf16[2048,64]{0,1:T(8,128)(2,1)S(1)}, bf16[2048,64]{0,1:T(8,128)(2,1)}, u32[]{:S(2)}) copy-start(bf16[2048,64]{0,1:T(8,128)(2,1)} %param.37) | copy-start | bytes 786436
  6.5 15.9 %copy-start.2 = (bf16[128,256]{1,0:T(8,128)(2,1)S(1)}, bf16[128,256]{1,0:T(8,128)(2,1)}, u32[]{:S(2)}) copy-start(bf16[128,256]{1,0:T(8,128)(2,1)} %param.31) | copy-start | bytes 196612
  6.5 24.4 %copy-start.3 = (bf16[128,256]{1,0:T(8,128)(2,1)S(1)}, bf16[128,256]{1,0:T(8,128)(2,1)}, u32[]{:S(2)}) copy-start(bf16[128,256]{1,0:T(8,128)(2,1)} %param.26) | copy-start | bytes 196612
  6.5 80.6 %all-gather.20.cloned.1.call-start = ((), (), s32[]{:S(2)}) async-start(), calls=%async_computation.5 | async-start | bytes 1310720 | tf_op jit(solution)/shard_map/all_gather | solution.py:159
  14.5 24.4 %copy-start.4 = (bf16[128,256]{1,0:T(8,128)(2,1)S(1)}, bf16[128,256]{1,0:T(8,128)(2,1)}, u32[]{:S(2)}) copy-start(bf16[128,256]{1,0:T(8,128)(2,1)} %param.27) | copy-start | bytes 196612
  14.5 74.6 %all-gather.24.cloned.1.call-start = ((), (), s32[]{:S(2)}) async-start(), calls=%async_computation.7 | async-start | bytes 1310720 | tf_op jit(solution)/shard_map/all_gather | solution.py:158
  22.4 24.1 %copy-start.5 = (bf16[128,256]{1,0:T(8,128)(2,1)S(1)}, bf16[128,256]{1,0:T(8,128)(2,1)}, u32[]{:S(2)}) copy-start(bf16[128,256]{1,0:T(8,128)(2,1)} %param.25) | copy-start | bytes 196612
  22.4 80.2 %all-gather.22.cloned.1.call-start = ((), (), s32[]{:S(2)}) async-start(), calls=%async_computation.6 | async-start | bytes 1310720 | tf_op jit(solution)/shard_map/all_gather | solution.py:160
  30.9 23.6 %copy-start.6 = (bf16[256,128]{1,0:T(8,128)(2,1)S(1)}, bf16[256,128]{1,0:T(8,128)(2,1)}, u32[]{:S(2)}) copy-start(bf16[256,128]{1,0:T(8,128)(2,1)} %param.40) | copy-start | bytes 196612
  30.9 211.9 %all-gather.14.cloned.1.call-start = ((), (), s32[]{:S(2)}) async-start(), calls=%async_computation.2 | async-start | bytes 1310720 | tf_op jit(solution)/shard_map/all_gather | solution.py:156
  38.8 23.5 %copy-start.7 = (bf16[256,128]{1,0:T(8,128)(2,1)S(1)}, bf16[256,128]{1,0:T(8,128)(2,1)}, u32[]{:S(2)}) copy-start(bf16[256,128]{1,0:T(8,128)(2,1)} %param.41) | copy-start | bytes 196612
  38.8 205.7 %all-gather.16.cloned.1.call-start = ((), (), s32[]{:S(2)}) async-start(), calls=%async_computation.3 | async-start | bytes 1310720 | tf_op jit(solution)/shard_map/all_gather | solution.py:157
  46.5 23.8 %copy-start.1 = (bf16[1,128,1024]{2,1,0:T(8,128)(2,1)S(1)}, bf16[1,128,1024]{2,1,0:T(8,128)(2,1)}, u32[]{:S(2)}) copy-start(bf16[1,128,1024]{2,1,0:T(8,128)(2,1)} %param.23) | copy-start | bytes 786436
  46.5 203.4 %all-gather.12.cloned.1.call-start = ((), (), s32[]{:S(2)}) async-start(), calls=%async_computation.1 | async-start | bytes 1310720 | tf_op jit(solution)/shard_map/all_gather | solution.py:155
  54.4 195.5 %all-gather.18.cloned.1.call-start = ((), (), s32[]{:S(2)}) async-start(), calls=%async_computation.4 | async-start | bytes 1310720 | tf_op jit(solution)/shard_map/all_gather | solution.py:239
  62.2 23.0 %copy-start.8 = (f32[2048]{0:T(1024)S(1)}, f32[2048]{0:T(1024)}, u32[]{:S(2)}) copy-start(f32[2048]{0:T(1024)} %param.24) | copy-start | bytes 24580
  62.2 23.0 %copy-start.13 = (bf16[64,256]{1,0:T(8,128)(2,1)S(1)}, bf16[64,256]{1,0:T(8,128)(2,1)}, u32[]{:S(2)}) copy-start(bf16[64,256]{1,0:T(8,128)(2,1)} %param.38) | copy-start | bytes 98308
  62.2 23.0 %copy-start.15 = (f32[256]{0:T(256)S(1)}, f32[256]{0:T(256)}, u32[]{:S(2)}) copy-start(f32[256]{0:T(256)} %param.36) | copy-start | bytes 3076
  62.2 191.2 %all-gather.26.cloned.1.call-start = ((), (), s32[]{:S(2)}) async-start(), calls=%async_computation.8 | async-start | bytes 1310720 | tf_op jit(solution)/shard_map/all_gather | solution.py:240
  70.2 201.0 %reduce-scatter.2.cloned.1.call-start = ((), (), s32[]{:S(2)}) async-start(), calls=%async_computation.9 | async-start | bytes 786432 | tf_op jit(solution)/shard_map/reduce_scatter | solution.py:244
  85.1 1.0 copy-start.12
  85.1 1.0 copy-start.14
  85.1 0.9 copy-start.16
  86.1 0.8 copy-start.10
  86.1 0.9 copy-start.9
  246.1 4.9 %collective-permute-start = (f32[2,256]{1,0:T(2,128)S(1)}, f32[2,256]{1,0:T(2,128)S(1)}, u32[]{:S(2)}, u32[]{:S(2)}) collective-permute-start(f32[2,256]{1,0:T(2,128)S(1)} %slice.51), channel_id=1, source_target_pairs={{0,8},{8,16},{16,24},{1,9},{9,17},{17,25},{2,10},{10,18},{18,26},{... | collective-permute-start | bytes 6152 | tf_op jit(solution)/shard_map/ppermute | solution.py:18
  251.0 2.4 copy-start.11
Sparse Core Ops, SparseCore 0:
  14.7 29.9 all-gather.19
  46.3 27.3 all-gather.23
  75.2 27.3 all-gather.21
  104.0 27.3 all-gather.13
  132.8 28.1 all-gather.15
  162.4 27.5 all-gather.11
  191.5 27.5 all-gather.17
  220.7 32.0 all-gather.25
  255.9 15.2 reduce-scatter.1
where the time goes:
time: 279 us; the launch traced here: 278 us
  blocking collectives  102 us (37%)
  matrix products  85.6 us (31%)
  other arithmetic  41.1 us (15%)
  waiting for transfers between devices  28.4 us (10%)
  between operations  13.7 us (5%)
  local copies, waits for them, and re-layouts  3.01 us (1%)
    another operation x20, other arithmetic, block_step(): lax.linalg.triangular_solve(unit_matrix - link_ab, rhs_terms, left_side=T...  39.8 us
    all_gather x2, blocking collectives, carried_in(): lax.all_gather(part.astype(kind), axis)  24.7 us
    dot_general x4, matrix products, block_step(): jnp.einsum('htc,htsc,hsc->hts', remove_dir, damp_prior, key_rate, precisi...  15.4 us
    reduce_scatter x1, waiting for transfers between devices, body(): lax.psum_scatter((jnp.dot(conv_out, conv_cols, preferred_element_type=jnp...  15.4 us
    dot_general x4, matrix products, block_step(): jnp.einsum('htc,htsc,hsc->hts', receive, damp_now, key_rate, precision=HI...  15.3 us
    dot_general x4, matrix products, block_step(): jnp.einsum('htc,htsc,hsc->hts', receive, damp_now, write_dir, precision=H...  15.3 us
    dot_general x4, matrix products, block_step(): jnp.einsum('htc,htsc,hsc->hts', remove_dir, damp_prior, write_dir, precis...  15.3 us
    all_gather x1, blocking collectives, body(): lax.all_gather(own_half, 'tp', axis=1, tiled=True).astype(jnp.float32)  14.6 us
  transfers between devices with their start and end apart: 10, of which 3 were waited for; matrix products, arithmetic and copies ran while one was open for 46% of the time, Pallas kernels for 0%

commit v1 on v0

--- a/solution.py
+++ b/solution.py
@@ -3,13 +3,17 @@
 
 import jax
 import jax.numpy as jnp
+import numpy as np
 from jax import lax
+from jax.experimental import pallas as pl
+from jax.experimental.pallas import tpu as pltpu
 from jax.sharding import PartitionSpec as P
 
 RMS_EPS = 1e-05
 GROUP_EPS = 0.00064
 UNIT_EPS = 1e-06
 HIGHEST = lax.Precision.HIGHEST
+MESH = pl.DeviceIdType.MESH
 
 
 def from_behind(array, axis, by):
@@ -252,6 +256,386 @@
     ).astype(jnp.float32)
     return merged.astype(jnp.bfloat16).reshape(1, own_rows, merged.shape[1])
 
+def mm(x, y, dims=(1, 0)):
+    xh = x.astype(jnp.bfloat16)
+    xl = (x - xh.astype(jnp.float32)).astype(jnp.bfloat16)
+    yh = y.astype(jnp.bfloat16)
+    yl = (y - yh.astype(jnp.float32)).astype(jnp.bfloat16)
+    how = (((dims[0],), (dims[1],)), ((), ()))
+
+    def one(p, q):
+        return lax.dot_general(p, q, how, preferred_element_type=jnp.float32)
+
+    return one(xh, yh) + (one(xh, yl) + one(xl, yh))
+
+
+def range_rows(length):
+    t = np.arange(length)[:, None]
+    u = np.arange(length)[None, :]
+    rows = []
+    h = 1
+    while h < length:
+        start = t // h * h
+        odd = (t // h) % 2 == 1
+        rows.append(np.where(odd, (u >= start) & (u < t), (u > t) & (u < start + h)))
+        rows.append(np.where(odd, (u >= start) & (u <= t), False))
+        h *= 2
+    rows.append(u < t)
+    rows.append(u <= t)
+    rows.append(u > t)
+    rows.append(np.ones((length, length), bool))
+    stacked = np.concatenate(rows, axis=0).astype(np.float32)
+    return np.concatenate([stacked] * 3, axis=1)
+
+
+def recur_kernel(
+    length, group, ld_ref, a_ref, b_ref, k_ref, r_ref, v_ref, sel_ref, gain_ref, out_ref,
+    t_buf, g_buf, q_buf, o_buf
+):
+    L = length
+    size = ld_ref.shape[1]
+    blocks = ld_ref.shape[0] // L
+    levels = L.bit_length() - 1
+    it = lax.broadcasted_iota(jnp.int32, (L, L), 0)
+    iu = lax.broadcasted_iota(jnp.int32, (L, L), 1)
+
+    def pair_mask(lv):
+        bt = lax.shift_right_logical(it, lv)
+        bu = lax.shift_right_logical(iu, lv)
+        return ((bt & 1) == 1) & (bu == bt - 1)
+
+    eye = jnp.where(it == iu, 1.0, 0.0).astype(jnp.float32)
+    ek_t = lax.broadcasted_iota(jnp.int32, (size, size), 0)
+    ek_u = lax.broadcasted_iota(jnp.int32, (size, size), 1)
+
+    def chunk_group(i, _):
+        base = [(i * group + g) for g in range(group)]
+        at = [pl.ds(pl.multiple_of(n * L, L), L) for n in base]
+        ld = [ld_ref[s, :] for s in at]
+        a = [a_ref[s, :] for s in at]
+        b = [b_ref[s, :] for s in at]
+        k = [k_ref[s, :] for s in at]
+        r = [r_ref[s, :] for s in at]
+        v = [v_ref[s, :] for s in at]
+        ex = []
+        for x in ld:
+            hi = x.astype(jnp.bfloat16)
+            rest = x - hi.astype(jnp.float32)
+            mid = rest.astype(jnp.bfloat16)
+            low = (rest - mid.astype(jnp.float32)).astype(jnp.bfloat16)
+            three = jnp.concatenate([hi, mid, low], axis=0)
+            ex.append(jnp.exp(jnp.dot(sel_ref[...], three, preferred_element_type=jnp.float32)))
+        acc_b = [None] * group
+        acc_k = [None] * group
+        for lv in range(levels + 1):
+            if lv < levels:
+                one = pair_mask(lv)
+                mask = jnp.concatenate([one, one], axis=0)
+            else:
+                mask = jnp.concatenate([jnp.zeros((L, L), jnp.float32), eye], axis=0) > 0.5
+            for g in range(group):
+                if lv < levels:
+                    e0 = ex[g][2 * lv * L : (2 * lv + 1) * L]
+                    e1 = ex[g][(2 * lv + 1) * L : (2 * lv + 2) * L]
+                    left = jnp.concatenate([a[g] * e0, r[g] * e1], axis=0)
+                    qb, qk = b[g] * e0, k[g] * e0
+                else:
+                    left = jnp.concatenate([a[g], r[g]], axis=0)
+                    qb, qk = b[g], k[g]
+                sb = jnp.where(mask, mm(left, qb, (1, 1)), 0.0)
+                sk = jnp.where(mask, mm(left, qk, (1, 1)), 0.0)
+                acc_b[g] = sb if lv == 0 else acc_b[g] + sb
+                acc_k[g] = sk if lv == 0 else acc_k[g] + sk
+        inv = [eye + jnp.where(pair_mask(0), acc_b[g][:L], 0.0) for g in range(group)]
+        for lv in range(1, levels):
+            mask = pair_mask(lv)
+            mid = [mm(inv[g], jnp.where(mask, acc_b[g][:L], 0.0)) for g in range(group)]
+            inv = [inv[g] + mm(mid[g], inv[g]) for g in range(group)]
+        tail = 2 * levels * L
+        for g in range(group):
+            e_ex = ex[g][tail : tail + L]
+            e_in = ex[g][tail + L : tail + 2 * L]
+            e_end = ex[g][tail + 2 * L : tail + 3 * L]
+            e_all = ex[g][tail + 3 * L : tail + 3 * L + size]
+            w = mm(inv[g], a[g] * e_ex)
+            u = mm(inv[g], mm(acc_k[g][:L], v[g]))
+            b_end = b[g] * e_end
+            n = base[g]
+            t_buf[n] = jnp.where(ek_t == ek_u, e_all, 0.0) + mm(b_end, w, (0, 0))
+            g_buf[n] = mm(b_end, u, (0, 0)) + mm(k[g] * e_end, v[g], (0, 0))
+            q_buf[n] = r[g] * e_in + mm(acc_b[g][L:], w)
+            o_buf[n] = mm(acc_b[g][L:], u) + mm(acc_k[g][L:], v[g])
+        return 0
+
+    lax.fori_loop(0, blocks // group, chunk_group, 0)
+
+    def pass_on(n, state):
+        read = mm(q_buf[n], state) + o_buf[n]
+        centred = read - jnp.mean(read, axis=-1, keepdims=True)
+        variance = jnp.mean(centred * centred, axis=-1, keepdims=True)
+        done = centred * lax.rsqrt(variance + GROUP_EPS) * gain_ref[...]
+        out_ref[pl.ds(pl.multiple_of(n * L, L), L), :] = done.astype(out_ref.dtype)
+        return mm(t_buf[n], state) + g_buf[n]
+
+    lax.fori_loop(0, blocks, pass_on, jnp.zeros((size, size), jnp.float32))
+
+
+def recurrence(log_decay, remove, write, key_rate, recv, vals, gain):
+    count, size = log_decay.shape
+    length = 64
+    blocks = count // length
+    group = 2 if blocks % 2 == 0 else 1
+    sel = jnp.asarray(range_rows(length), jnp.bfloat16)
+    vm = pl.BlockSpec(memory_space=pltpu.VMEM)
+    return pl.pallas_call(
+        partial(recur_kernel, length, group),
+        out_shape=jax.ShapeDtypeStruct((count, size), jnp.bfloat16),
+        in_specs=[vm] * 8,
+        out_specs=vm,
+        scratch_shapes=[
+            pltpu.VMEM((blocks, size, size), jnp.float32),
+            pltpu.VMEM((blocks, size, size), jnp.float32),
+            pltpu.VMEM((blocks, length, size), jnp.float32),
+            pltpu.VMEM((blocks, length, size), jnp.float32),
+        ],
+    )(log_decay, remove, write, key_rate, recv, vals, sel, gain.reshape(1, size))
+
+
+def peers():
+    sp, fs, tp = (lax.axis_size(name) for name in ("sp", "fs", "tp"))
+    z, f, c = (lax.axis_index(name) for name in ("sp", "fs", "tp"))
+    return sp, fs, tp, z, f, c
+
+
+def greet(devices):
+    barrier = pltpu.get_barrier_semaphore()
+    for device in devices:
+        pl.semaphore_signal(barrier, inc=1, device_id=device, device_id_type=MESH)
+    pl.semaphore_wait(barrier, len(devices))
+
+
+def send(src, dst, sends, recvs, device):
+    copy = pltpu.make_async_remote_copy(
+        src_ref=src, dst_ref=dst, send_sem=sends, recv_sem=recvs,
+        device_id=device, device_id_type=MESH,
+    )
+    copy.start()
+    return copy
+
+
+def gather_kernel(
+    tok_ref, w_ref, o_ref, shift_ref, toks, weights, outs, shifts,
+    loc_sem, zs, zr, fs_s, fs_r, ts, tr, ps, pr, hs, hr, ozs, ozr, ofs, ofr, ops, opr
+):
+    sp, fs, tp, z, f, c = peers()
+    across = [lax.rem(z + d, sp) for d in range(sp)]
+    behind = [lax.rem(z + sp - d, sp) for d in range(sp)]
+    beside = [lax.rem(f + d, fs) for d in range(fs)]
+    other = 1 - c
+    zdev = [(across[d], f, c) for d in range(sp)]
+    fdev = [(z, beside[d], c) for d in range(fs)]
+    partner = (z, f, other)
+    rows, feats = tok_ref.shape
+    orows, ocols = o_ref.shape
+    greet(zdev[1:] + fdev[1:] + [partner])
+
+    def tok_at(zi, ci):
+        return toks.at[pl.ds(pl.multiple_of(zi * rows, rows), rows),
+                       pl.ds(pl.multiple_of(ci * feats, feats), feats)]
+
+    def out_at(zi, fi, ci):
+        return outs.at[pl.ds(pl.multiple_of(ci * orows, orows), orows),
+                       pl.ds(pl.multiple_of((zi * fs + fi) * ocols, ocols), ocols)]
+
+    local = [
+        pltpu.make_async_copy(w_ref.at[z], weights.at[z, f], loc_sem.at[0]),
+        pltpu.make_async_copy(tok_ref, tok_at(z, c), loc_sem.at[1]),
+        pltpu.make_async_copy(shift_ref.at[z], shifts.at[z], loc_sem.at[2]),
+        pltpu.make_async_copy(o_ref, out_at(z, f, c), loc_sem.at[3]),
+    ]
+    for copy in local:
+        copy.start()
+    w_z = [send(w_ref.at[across[d]], weights.at[z, f], zs.at[d], zr.at[d], zdev[d])
+           for d in range(1, sp)]
+    s_z = [send(shift_ref.at[across[d]], shifts.at[z], hs.at[d], hr.at[d], zdev[d])
+           for d in range(1, sp)]
+    w_f = [send(w_ref.at[z], weights.at[z, f], fs_s.at[0, e], fs_r.at[0, e], fdev[e])
+           for e in range(1, fs)]
+    t_p = [send(tok_ref, tok_at(z, c), ps.at[0], pr.at[0], partner)]
+    t_z = [send(tok_ref, tok_at(z, c), ts.at[d], tr.at[d], zdev[d]) for d in range(1, sp)]
+    o_z = [send(o_ref, out_at(z, f, c), ozs.at[d], ozr.at[d], zdev[d]) for d in range(1, sp)]
+    for d in range(1, sp):
+        w_z[d - 1].wait_recv()
+        got = weights.at[behind[d], f]
+        w_f += [send(got, got, fs_s.at[d, e], fs_r.at[d, e], fdev[e]) for e in range(1, fs)]
+    o_f = [send(o_ref, out_at(z, f, c), ofs.at[0, e], ofr.at[0, e], fdev[e])
+           for e in range(1, fs)]
+    o_p = [send(o_ref, out_at(z, f, c), ops.at[0, 0], opr.at[0, 0], partner)]
+    for d in range(1, sp):
+        t_z[d - 1].wait_recv()
+        got = tok_at(behind[d], c)
+        t_p.append(send(got, got, ps.at[d], pr.at[d], partner))
+    for d in range(1, sp):
+        o_z[d - 1].wait_recv()
+        got = out_at(behind[d], f, c)
+        o_f += [send(got, got, ofs.at[d, e], ofr.at[d, e], fdev[e]) for e in range(1, fs)]
+        o_p.append(send(got, got, ops.at[d, 0], opr.at[d, 0], partner))
+    for d in range(sp):
+        for e in range(1, fs):
+            o_f[d * (fs - 1) + e - 1].wait_recv()
+            got = out_at(behind[d], lax.rem(f + fs - e, fs), c)
+            o_p.append(send(got, got, ops.at[d, e], opr.at[d, e], partner))
+    for copy in local:
+        copy.wait()
+    for copy in w_z + t_z + o_z + o_f:
+        copy.wait_send()
+    for copy in s_z + w_f + t_p + o_p:
+        copy.wait()
+
+
+def gather_all(tok, w, o, shift):
+    sp, fs, tp = (lax.axis_size(name) for name in ("sp", "fs", "tp"))
+    vm = pl.BlockSpec(memory_space=pltpu.VMEM)
+    dma = pltpu.SemaphoreType.DMA
+    rows, feats = tok.shape
+    return pl.pallas_call(
+        gather_kernel,
+        out_shape=(
+            jax.ShapeDtypeStruct((sp * rows, tp * feats), tok.dtype),
+            jax.ShapeDtypeStruct((sp, fs) + w.shape[1:], w.dtype),
+            jax.ShapeDtypeStruct((tp * o.shape[0], sp * fs * o.shape[1]), o.dtype),
+            jax.ShapeDtypeStruct(shift.shape, shift.dtype),
+        ),
+        in_specs=[vm] * 4,
+        out_specs=(vm,) * 4,
+        scratch_shapes=[
+            dma((4,)), dma((sp,)), dma((sp,)), dma((sp, fs)), dma((sp, fs)), dma((sp,)), dma((sp,)),
+            dma((sp,)), dma((sp,)), dma((sp,)), dma((sp,)), dma((sp,)), dma((sp,)),
+            dma((sp, fs)), dma((sp, fs)), dma((sp, fs)), dma((sp, fs)),
+        ],
+        compiler_params=pltpu.CompilerParams(collective_id=0, has_side_effects=True),
+    )(tok, w, o, shift)
+
+
+def swap_kernel(act_ref, got_ref, loc_sem, sends, recvs):
+    sp, fs, tp, z, f, c = peers()
+    rows = act_ref.shape[0] // (sp * tp)
+    cols = act_ref.shape[1]
+    steps = [(d, e) for d in range(sp) for e in range(tp)]
+    dest = [(lax.rem(z + d, sp), lax.rem(c + e, tp)) for d, e in steps]
+    greet([(dz, f, dc) for dz, dc in dest[1:]])
+
+    def piece(dz, dc):
+        return act_ref.at[pl.ds(pl.multiple_of((dz * tp + dc) * rows, rows), rows)]
+
+    mine = got_ref.at[:, pl.ds(pl.multiple_of((c * sp + z) * cols, cols), cols)]
+    own = pltpu.make_async_copy(piece(z, c), mine, loc_sem)
+    own.start()
+    copies = [send(piece(dz, dc), mine, sends.at[i], recvs.at[i], (dz, f, dc))
+              for i, (dz, dc) in enumerate(dest) if i]
+    own.wait()
+    for copy in copies:
+        copy.wait()
+
+
+def swap_all(act):
+    sp, tp = (lax.axis_size(name) for name in ("sp", "tp"))
+    vm = pl.BlockSpec(memory_space=pltpu.VMEM)
+    return pl.pallas_call(
+        swap_kernel,
+        out_shape=jax.ShapeDtypeStruct(
+            (act.shape[0] // (sp * tp), act.shape[1] * sp * tp), act.dtype
+        ),
+        in_specs=[vm],
+        out_specs=vm,
+        scratch_shapes=[
+            pltpu.SemaphoreType.DMA,
+            pltpu.SemaphoreType.DMA((sp * tp,)),
+            pltpu.SemaphoreType.DMA((sp * tp,)),
+        ],
+        compiler_params=pltpu.CompilerParams(collective_id=1, has_side_effects=True),
+    )(act)
+
+
+def head_body(
+    tokens, norm_gain, conv_gate_out, conv_gate_in, conv_value, conv_taps, recv_weight,
+    key_weight, value_weight, decay_base, decay_down, decay_up, decay_shift, rate_base,
+    rate_down, rate_up, head_gain, out_conv, out_state,
+):
+    sp = lax.axis_size("sp")
+    z = lax.axis_index("sp")
+    tok_count = tokens.shape[1]
+    size = recv_weight.shape[1] // sp
+    own_rows = conv_gate_out.shape[0]
+    tok = tokens.reshape(tok_count, tokens.shape[2])
+    six = (conv_gate_out, conv_gate_in, conv_value, recv_weight, key_weight, value_weight)
+    split = jnp.stack([m.reshape(own_rows, sp, size) for m in six], axis=2)
+    w = split.transpose(1, 0, 2, 3).reshape(sp, own_rows, 6 * size)
+    o_cols = out_conv.shape[1]
+    o = jnp.stack(
+        [out_conv.reshape(sp, size, o_cols), out_state.reshape(sp, size, o_cols)], axis=1
+    ).reshape(2 * sp * size, o_cols)
+    shift = decay_shift.reshape(tok_count, sp).T.reshape(sp, 1, tok_count)
+    toks, weights, outs, shifts = gather_all(tok, w, o, shift)
+    features = toks.astype(jnp.float32)
+    normed = (
+        features
+        * lax.rsqrt(jnp.mean(features * features, axis=-1, keepdims=True) + RMS_EPS)
+        * norm_gain
+    ).astype(jnp.bfloat16)
+    all_w = weights.reshape(toks.shape[1], 6 * size)
+    low_w = jnp.concatenate([decay_down, rate_down], axis=1)
+    proj = jnp.dot(normed, all_w, preferred_element_type=jnp.float32).astype(jnp.bfloat16)
+    lows = jnp.dot(normed, low_w, preferred_element_type=jnp.float32)
+    gate_out, gate_in, conv_in, recv, keys, vals = (
+        proj[:, i * size : (i + 1) * size].astype(jnp.float32) for i in range(6)
+    )
+    inner = decay_down.shape[1]
+    decay_low = jnp.tanh(lows[:, :inner]).astype(jnp.bfloat16)
+    rate_low = lows[:, inner:].astype(jnp.bfloat16)
+
+    def mine(array):
+        return lax.dynamic_slice_in_dim(array, z * size, size, axis=array.ndim - 1)
+
+    decay_pre = mine(decay_base) + jnp.dot(
+        decay_low, mine(decay_up), preferred_element_type=jnp.float32
+    )
+    log_base = -jax.nn.softplus(-decay_pre) - 0.5
+    log_decay = -jnp.exp(log_base + shifts.reshape(sp * tok_count, 1))
+    rate = jax.nn.sigmoid(
+        mine(rate_base) + jnp.dot(rate_low, mine(rate_up), preferred_element_type=jnp.float32)
+    )
+    unit = keys * lax.rsqrt(jnp.sum(keys * keys, axis=-1, keepdims=True) + UNIT_EPS)
+    state_out = recurrence(
+        log_decay, -unit, unit * rate, keys * rate, recv, vals, mine(head_gain)
+    )
+    mixed_in = gate_in * conv_in
+    total = mixed_in.shape[0]
+    padded = jnp.pad(mixed_in, ((2, 0), (0, 0)))
+    taps = mine(conv_taps)
+    convolved = (
+        padded[:total] * taps[0] + padded[1 : total + 1] * taps[1] + padded[2:] * taps[2]
+    )
+    conv_out = (gate_out * convolved).astype(jnp.bfloat16)
+    act = swap_all(jnp.concatenate([conv_out, state_out], axis=1))
+    mixed = jnp.dot(act, outs, preferred_element_type=jnp.float32).astype(jnp.bfloat16)
+    return mixed.reshape((1,) + mixed.shape)
+
+
+def one_head_each(mesh, tokens, shift, weight):
+    sp, tp = mesh.shape["sp"], mesh.shape["tp"]
+    heads = shift.shape[2]
+    count = tokens.shape[1] // sp
+    size = weight.shape[1] // heads
+    return (
+        tp == 2
+        and heads == sp * tp
+        and tokens.shape[0] == mesh.shape["fs"]
+        and size == 64
+        and count % 128 == 0
+        and weight.shape[0] % (sp * mesh.shape["fs"] * 16) == 0
+    )
+
 
 def solution(mesh):
     placed = (
@@ -275,6 +659,11 @@
         P("tp", ("sp", "fs")),
         P("tp", ("sp", "fs")),
     )
-    return jax.shard_map(
-        body, mesh=mesh, in_specs=placed, out_specs=P("fs", ("sp", "tp"), None), check_vma=False
-    )
+    def run(*args):
+        chosen = head_body if one_head_each(mesh, args[0], args[12], args[6]) else body
+        return jax.shard_map(
+            chosen, mesh=mesh, in_specs=placed, out_specs=P("fs", ("sp", "tp"), None),
+            check_vma=False,
+        )(*args)
+
+    return run

time: 279 us -> 120 us (0.43)
  blocking collectives: 102 us -> 0 us
  Pallas kernels: 0 us -> 92.9 us
  matrix products: 85.6 us -> 10.6 us
  other arithmetic: 41.1 us -> 6.44 us
  waiting for transfers between devices: 28.4 us -> 0 us
  between operations: 13.7 us -> 0.24 us
  local copies, waits for them, and re-layouts: 3.01 us -> 7.66 us
    all_gather x11 -> x0, blocking collectives: 102 us -> none  [the longest x2 24.7 us: carried_in(): lax.all_gather(part.astype(kind), axis)]
    pallas_call x0 -> x3, Pallas kernels: none -> 92.9 us  [the longest x1 66.3 us: gather_all(): pl.pallas_call(gather_kernel, out_shape=(jax.ShapeDtypeStruct((sp * rows,...]
    dot_general x58 -> x5, matrix products: 84.5 us -> 10.6 us  [the longest x1 3.82 us: head_body(): jnp.dot(act, outs, preferred_element_type=jnp.float32).astype(jnp.bfloat16)]
    another operation x24 -> x1, other arithmetic: 40.1 us -> 1.54 us  [head_body(): jnp.stack([out_conv.reshape(sp, size, o_cols), out_state.reshape(sp, size...]
    reduce_scatter x1 -> x0, waiting for transfers between devices: 15.4 us -> none  [body(): lax.psum_scatter((jnp.dot(conv_out, conv_cols, preferred_element_type=jnp...]
    all_gather x8 -> x0, waiting for transfers between devices: 11.8 us -> none  [the longest x1 11.7 us: body(): lax.all_gather(local_vw, 'sp', axis=0, tiled=True)]
    unnamed x34 -> x33, local copies, waits for them, and re-layouts: 0.16 us -> 5.85 us
  transfers between devices with their start and end apart: 10 -> 0, of which waited for: 3 -> 0; matrix products, arithmetic and copies ran while one was open for 46% -> 0% of each run, Pallas kernels for 0% -> 0%
where the time goes in v1:
time: 120 us; the launch traced here: 118 us
  Pallas kernels  92.9 us (77%)
  matrix products  10.6 us (9%)
  local copies, waits for them, and re-layouts  7.66 us (6%)
  other arithmetic  6.44 us (5%)
    pallas_call x1, Pallas kernels, gather_all(): pl.pallas_call(gather_kernel, out_shape=(jax.ShapeDtypeStruct((sp * rows,...  66.3 us
    pallas_call x1, Pallas kernels, recurrence(): pl.pallas_call(partial(recur_kernel, length, group), out_shape=jax.ShapeD...  17.7 us
    pallas_call x1, Pallas kernels, swap_all(): pl.pallas_call(swap_kernel, out_shape=jax.ShapeDtypeStruct((act.shape[0]...  8.92 us
    unnamed x33, local copies, waits for them, and re-layouts  5.85 us
    dot_general x1, matrix products, head_body(): jnp.dot(act, outs, preferred_element_type=jnp.float32).astype(jnp.bfloat16)  3.82 us
    dot_general x1, matrix products, head_body(): jnp.dot(normed, all_w, preferred_element_type=jnp.float32)  3.48 us

profile of v1, /device:TPU:11, one launch (start us, length us, event | category | flops | bytes accessed | tf_op | source)
XLA Modules:
  0.0 117.8 jit_solution(13488301397075112209)
XLA Ops:
  0.0 0.0 copy-start
  0.0 0.0 copy-start.6
  0.0 1.0 copy.45
  1.0 1.0 copy.46
  2.0 1.0 copy.47
  2.9 1.0 copy.48
  3.9 1.0 copy.49
  4.9 1.0 copy.50
  5.9 1.0 copy.54.w_ref
  6.9 1.5 %pad_maximum_fusion = bf16[4,2,64,128]{3,2,1,0:T(8,128)(2,1)} fusion(bf16[4,1,64,128]{3,2,1,0:T(8,128)(2,1)} %bitcast.46, bf16[4,1,64,128]{3,2,1,0:T(8,128)(2,1)} %bitcast.47), kind=kLoop, calls=%fused_computation.38 | loop fusion | flops 65536 | bytes 262144 | tf_op jit(solution)/shard_map/stack | solution.py:575
  8.4 66.3 %shard_map.190 = (bf16[512,2048]{1,0:T(8,128)(2,1)}, bf16[4,4,128,384]{3,2,1,0:T(8,128)(2,1)}, bf16[1024,2048]{1,0:T(8,128)(2,1)}, f32[4,1,128]{2,1,0:T(1,128)}) custom-call(bf16[128,1024]{1,0:T(8,128)(2,1)} %bitcast.39, bf16[4,128,384]{2,1,0:T(8,128)(2,1)} %copy.54.w_ref, bf16[512,128]{1,0:T(8,128)(2,1)} %bitcast.38, f32[4,1,128]{2,1,0:T(1,128)} %bitcast.48), custom_call_target="tpu_custom_call" | custom-call | tf_op jit(solution)/shard_map/pallas_call | solution.py:501
  74.7 2.1 %fusion = f32[512]{0:T(512)S(1)} fusion(bf16[512,2048]{1,0:T(8,128)(2,1)} %get-tuple-element.9), kind=kLoop, calls=%fused_computation.2 | loop fusion | flops 3145216 | bytes 2099200 | tf_op jit(solution)/shard_map/reduce_sum | solution.py:583
  76.8 0.0 copy-start.2
  76.8 0.0 copy-start.1
  76.8 0.0 copy-start.3
  76.8 0.0 copy-start.4
  76.8 0.0 copy-done.6
  76.9 3.5 %convolution_convert_fusion.1 = bf16[512,384]{1,0:T(8,128)(2,1)S(1)} fusion(bf16[2048,384]{1,0:T(8,128)(2,1)} %bitcast.49, bf16[512,2048]{1,0:T(8,128)(2,1)} %get-tuple-element.9, f32[2048]{0:T(1024)S(1)} %copy-done.6, f32[512]{0:T(512)S(1)} %add_rsqrt_fusion.1), kind=kOutput, calls=%fused_computation.7 | convolution fusion | flops 809697280 | bytes 4073472 | tf_op jit(solution)/shard_map/dot_general | solution.py:588
  80.3 0.0 copy-start.8
  80.4 0.0 copy-start.9
  80.4 0.0 copy-start.5
  80.4 0.0 copy-start.7
  80.4 0.2 convert_multiply_fusion.5
  80.6 0.0 copy-done.2
  80.6 0.1 constant_dynamic-slice_fusion
  80.7 0.0 copy-done.1
  80.7 0.0 copy-done.3
  80.7 0.0 copy-done.4
  80.7 0.0 copy-start.10
  80.7 0.9 fusion.9
  81.6 0.0 copy-done.8
  81.7 0.1 dynamic_slice.21
  81.7 0.0 copy-done
  81.7 1.3 %convert_multiply_fusion.2 = (f32[512,64]{1,0:T(8,128)}, f32[512,64]{1,0:T(8,128)}, f32[512,64]{1,0:T(8,128)}, bf16[512,64]{1,0:T(8,128)(2,1)S(1)}) fusion(bf16[512,384]{1,0:T(8,128)(2,1)S(1)} %convolution_convert_fusion.1, f32[512]{0:T(512)S(1)} %add_rsqrt_fusion, f32[512,64]{1,0:T(8,128)S(1)} %get-tuple-element.17, f32[64]{0:T(128)S(1)} %get-tuple-element.22, ...), kind=kOutput, calls=%fused_computation.20 | convolution fusion | flops 4751360 | bytes 1069060 | tf_op jit(solution)/shard_map/dot_general | solution.py:606
  83.0 0.0 copy-done.9
  83.0 0.1 dynamic_slice.19
  83.1 0.0 copy-done.5
  83.1 0.0 copy-done.7
  83.1 1.1 fusion.22.ld_ref
  84.2 0.9 slice_convert_fusion
  85.2 0.0 copy-done.10
  85.2 0.6 dynamic-slice_bitcast_fusion.gain_ref
  85.7 17.7 %shard_map.191 = bf16[512,64]{1,0:T(8,128)(2,1)} custom-call(f32[512,64]{1,0:T(8,128)} %fusion.22.ld_ref, f32[512,64]{1,0:T(8,128)} %get-tuple-element.15.a_ref, f32[512,64]{1,0:T(8,128)} %get-tuple-element.14.b_ref, f32[512,64]{1,0:T(8,128)} %get-tuple-element.13.k_ref, f32[512,64]{1,0:T(8,128)} %get-tuple-element.20.r_ref, ...), custom_call_target="tpu_custom_call" | custom-call | tf_op jit(solution)/shard_map/pallas_call | solution.py:390
  103.4 1.7 %pad_maximum_fusion.1.act_ref = bf16[512,128]{1,0:T(8,128)(2,1)} fusion(bf16[512,64]{1,0:T(8,128)(2,1)} %shard_map.191, bf16[512,64]{1,0:T(8,128)(2,1)S(1)} %get-tuple-element.16), kind=kLoop, calls=%fused_computation.39 | loop fusion | flops 262144 | bytes 262144 | tf_op jit(solution)/shard_map/concatenate | solution.py:620
  105.1 8.9 %shard_map.192 = bf16[64,1024]{1,0:T(8,128)(2,1)} custom-call(bf16[512,128]{1,0:T(8,128)(2,1)} %pad_maximum_fusion.1.act_ref), custom_call_target="tpu_custom_call" | custom-call | tf_op jit(solution)/shard_map/pallas_call | solution.py:544
  114.0 3.8 %fusion.3 = bf16[1,64,2048]{2,1,0:T(8,128)(2,1)} fusion(bf16[64,1024]{1,0:T(8,128)(2,1)} %shard_map.192, bf16[1024,2048]{1,0:T(8,128)(2,1)} %get-tuple-element.12), kind=kOutput, calls=%fused_computation.6 | convolution fusion | flops 268566528 | bytes 4587520 | tf_op jit(solution)/shard_map/dot_general | solution.py:621
  (10 shorter events, 0.1 us)
Async XLA Ops:
  0.0 81.7 %copy-start = (bf16[64,256]{1,0:T(8,128)(2,1)S(1)}, bf16[64,256]{1,0:T(8,128)(2,1)}, u32[]{:S(2)}) copy-start(bf16[64,256]{1,0:T(8,128)(2,1)} %param.35) | copy-start | bytes 98308
  0.0 76.8 %copy-start.6 = (f32[2048]{0:T(1024)S(1)}, f32[2048]{0:T(1024)}, u32[]{:S(2)}) copy-start(f32[2048]{0:T(1024)} %param.21) | copy-start | bytes 24580
  76.8 3.8 %copy-start.2 = (f32[3,256]{1,0:T(4,128)S(1)}, f32[3,256]{1,0:T(4,128)}, u32[]{:S(2)}) copy-start(f32[3,256]{1,0:T(4,128)} %param.25) | copy-start | bytes 9220
  76.8 3.9 %copy-start.1 = (bf16[512,2048]{1,0:T(8,128)(2,1)S(1)}, bf16[512,2048]{1,0:T(8,128)(2,1)}, u32[]{:S(2)}) copy-start(bf16[512,2048]{1,0:T(8,128)(2,1)} %get-tuple-element.9) | copy-start | bytes 6291460
  76.8 3.9 %copy-start.3 = (bf16[2048,64]{0,1:T(8,128)(2,1)S(1)}, bf16[2048,64]{0,1:T(8,128)(2,1)}, u32[]{:S(2)}) copy-start(bf16[2048,64]{0,1:T(8,128)(2,1)} %param.34) | copy-start | bytes 786436
  76.8 3.9 %copy-start.4 = (bf16[2048,64]{0,1:T(8,128)(2,1)S(1)}, bf16[2048,64]{0,1:T(8,128)(2,1)}, u32[]{:S(2)}) copy-start(bf16[2048,64]{0,1:T(8,128)(2,1)} %param.30) | copy-start | bytes 786436
  80.3 1.3 %copy-start.8 = (f32[256]{0:T(256)S(1)}, f32[256]{0:T(256)}, u32[]{:S(2)}) copy-start(f32[256]{0:T(256)} %param.33) | copy-start | bytes 3076
  80.4 2.7 %copy-start.9 = (f32[256]{0:T(256)S(1)}, f32[256]{0:T(256)}, u32[]{:S(2)}) copy-start(f32[256]{0:T(256)} %param.29) | copy-start | bytes 3076
  80.4 2.7 %copy-start.5 = (bf16[64,256]{1,0:T(8,128)(2,1)S(1)}, bf16[64,256]{1,0:T(8,128)(2,1)}, u32[]{:S(2)}) copy-start(bf16[64,256]{1,0:T(8,128)(2,1)} %param.31) | copy-start | bytes 98308
  80.4 2.7 %copy-start.7 = (f32[4,1,128]{2,1,0:T(1,128)S(1)}, f32[4,1,128]{2,1,0:T(1,128)}, u32[]{:S(2)}) copy-start(f32[4,1,128]{2,1,0:T(1,128)} %get-tuple-element.11) | copy-start | bytes 6148
  80.7 4.5 %copy-start.10 = (f32[256]{0:T(256)S(1)}, f32[256]{0:T(256)}, u32[]{:S(2)}) copy-start(f32[256]{0:T(256)} %param.36) | copy-start | bytes 3076

commit v2 on v0

--- a/solution.py
+++ b/solution.py
@@ -3,13 +3,17 @@
 
 import jax
 import jax.numpy as jnp
+import numpy as np
 from jax import lax
+from jax.experimental import pallas as pl
+from jax.experimental.pallas import tpu as pltpu
 from jax.sharding import PartitionSpec as P
 
 RMS_EPS = 1e-05
 GROUP_EPS = 0.00064
 UNIT_EPS = 1e-06
 HIGHEST = lax.Precision.HIGHEST
+MESH = pl.DeviceIdType.MESH
 
 
 def from_behind(array, axis, by):
@@ -252,6 +256,440 @@
     ).astype(jnp.float32)
     return merged.astype(jnp.bfloat16).reshape(1, own_rows, merged.shape[1])
 
+def mm(x, y, dims=(1, 0)):
+    xh = x.astype(jnp.bfloat16)
+    xl = (x - xh.astype(jnp.float32)).astype(jnp.bfloat16)
+    yh = y.astype(jnp.bfloat16)
+    yl = (y - yh.astype(jnp.float32)).astype(jnp.bfloat16)
+    how = (((dims[0],), (dims[1],)), ((), ()))
+
+    def one(p, q):
+        return lax.dot_general(p, q, how, preferred_element_type=jnp.float32)
+
+    return one(xh, yh) + (one(xh, yl) + one(xl, yh))
+
+
+def range_rows(length):
+    t = np.arange(length)[:, None]
+    u = np.arange(length)[None, :]
+    rows = []
+    h = 1
+    while h < length:
+        start = t // h * h
+        odd = (t // h) % 2 == 1
+        rows.append(np.where(odd, (u >= start) & (u < t), (u > t) & (u < start + h)))
+        rows.append(np.where(odd, (u >= start) & (u <= t), False))
+        h *= 2
+    rows.append(u < t)
+    rows.append(u <= t)
+    rows.append(u > t)
+    rows.append(np.ones((length, length), bool))
+    stacked = np.concatenate(rows, axis=0).astype(np.float32)
+    return np.concatenate([stacked] * 3, axis=1)
+
+
+def peers():
+    sp, fs, tp = (lax.axis_size(name) for name in ("sp", "fs", "tp"))
+    z, f, c = (lax.axis_index(name) for name in ("sp", "fs", "tp"))
+    return sp, fs, tp, z, f, c
+
+
+def greet(devices):
+    barrier = pltpu.get_barrier_semaphore()
+    for device in devices:
+        pl.semaphore_signal(barrier, inc=1, device_id=device, device_id_type=MESH)
+    pl.semaphore_wait(barrier, len(devices))
+
+
+def send(src, dst, sends, recvs, device):
+    copy = pltpu.make_async_remote_copy(
+        src_ref=src, dst_ref=dst, send_sem=sends, recv_sem=recvs,
+        device_id=device, device_id_type=MESH,
+    )
+    copy.start()
+    return copy
+
+
+def pair_mask(length, lv):
+    bt = lax.shift_right_logical(lax.broadcasted_iota(jnp.int32, (length, length), 0), lv)
+    bu = lax.shift_right_logical(lax.broadcasted_iota(jnp.int32, (length, length), 1), lv)
+    return ((bt & 1) == 1) & (bu == bt - 1)
+
+
+def unit_matrix(size):
+    it = lax.broadcasted_iota(jnp.int32, (size, size), 0)
+    iu = lax.broadcasted_iota(jnp.int32, (size, size), 1)
+    return jnp.where(it == iu, 1.0, 0.0).astype(jnp.float32)
+
+
+def blocks_of(first, group, L, fields, sel_ref, bufs):
+    t_buf, g_buf, q_buf, o_buf = bufs
+    levels = L.bit_length() - 1
+    base = [first + g for g in range(group)]
+    at = [pl.ds(pl.multiple_of(n * L, L), L) for n in base]
+    ld, a, b, k, r, v = ([ref[s, :] for s in at] for ref in fields)
+    size = ld[0].shape[1]
+    eye = unit_matrix(L)
+    ex = []
+    for x in ld:
+        hi = x.astype(jnp.bfloat16)
+        rest = x - hi.astype(jnp.float32)
+        mid = rest.astype(jnp.bfloat16)
+        low = (rest - mid.astype(jnp.float32)).astype(jnp.bfloat16)
+        three = jnp.concatenate([hi, mid, low], axis=0)
+        ex.append(jnp.exp(jnp.dot(sel_ref[...], three, preferred_element_type=jnp.float32)))
+    acc_b = [None] * group
+    acc_k = [None] * group
+    for lv in range(levels + 1):
+        if lv < levels:
+            one = pair_mask(L, lv)
+            mask = jnp.concatenate([one, one], axis=0)
+        else:
+            mask = jnp.concatenate([jnp.zeros((L, L), jnp.float32), eye], axis=0) > 0.5
+        for g in range(group):
+            if lv < levels:
+                e0 = ex[g][2 * lv * L : (2 * lv + 1) * L]
+                e1 = ex[g][(2 * lv + 1) * L : (2 * lv + 2) * L]
+                left = jnp.concatenate([a[g] * e0, r[g] * e1], axis=0)
+                qb, qk = b[g] * e0, k[g] * e0
+            else:
+                left = jnp.concatenate([a[g], r[g]], axis=0)
+                qb, qk = b[g], k[g]
+            sb = jnp.where(mask, mm(left, qb, (1, 1)), 0.0)
+            sk = jnp.where(mask, mm(left, qk, (1, 1)), 0.0)
+            acc_b[g] = sb if lv == 0 else acc_b[g] + sb
+            acc_k[g] = sk if lv == 0 else acc_k[g] + sk
+    inv = [eye + jnp.where(pair_mask(L, 0), acc_b[g][:L], 0.0) for g in range(group)]
+    for lv in range(1, levels):
+        mask = pair_mask(L, lv)
+        half = [mm(inv[g], jnp.where(mask, acc_b[g][:L], 0.0)) for g in range(group)]
+        inv = [inv[g] + mm(half[g], inv[g]) for g in range(group)]
+    tail = 2 * levels * L
+    for g in range(group):
+        e_ex = ex[g][tail : tail + L]
+        e_in = ex[g][tail + L : tail + 2 * L]
+        e_end = ex[g][tail + 2 * L : tail + 3 * L]
+        e_all = ex[g][tail + 3 * L : tail + 3 * L + size]
+        w = mm(inv[g], a[g] * e_ex)
+        u = mm(inv[g], mm(acc_k[g][:L], v[g]))
+        b_end = b[g] * e_end
+        n = base[g]
+        t_buf[n] = unit_matrix(size) * e_all + mm(b_end, w, (0, 0))
+        g_buf[n] = mm(b_end, u, (0, 0)) + mm(k[g] * e_end, v[g], (0, 0))
+        q_buf[n] = r[g] * e_in + mm(acc_b[g][L:], w)
+        o_buf[n] = mm(acc_b[g][L:], u) + mm(acc_k[g][L:], v[g])
+
+
+def sigmoid(x):
+    return jnp.exp(jnp.minimum(x, 0.0)) / (1.0 + jnp.exp(-jnp.abs(x)))
+
+
+def halves(tile):
+    size = tile.shape[1] // 2
+    return tile[:, :size], pltpu.roll(tile, size, 1)[:, :size]
+
+
+def layer_kernel(
+    tok_ref, go_ref, gi_ref, cv_ref, rw_ref, kw_ref, vw_ref, oc_ref, os_ref, shift_ref,
+    norm_ref, low_ref, up_ref, base_ref, taps_ref, gain_ref, sel_ref, out_ref,
+    toks, w_ref, weights, o_ref, outs, shifts, ld_ref, a_ref, b_ref, k_ref, r_ref, v_ref,
+    gate_ref, mixed_ref, t_buf, g_buf, q_buf, o_buf, act_ref, got_ref,
+    loc_sem, zs, zr, fs_s, fs_r, ts, tr, ps, pr, hs, hr, ozs, ozr, ofs, ofr, ops, opr,
+    act_s, act_r,
+):
+    sp, fs, tp, z, f, c = peers()
+    across = [lax.rem(z + d, sp) for d in range(sp)]
+    behind = [lax.rem(z + sp - d, sp) for d in range(sp)]
+    beside = [lax.rem(f + d, fs) for d in range(fs)]
+    other = 1 - c
+    zdev = [(across[d], f, c) for d in range(sp)]
+    fdev = [(z, beside[d], c) for d in range(fs)]
+    partner = (z, f, other)
+    rows, feats = tok_ref.shape
+    orows, ocols = o_ref.shape
+    wide = 2 * (go_ref.shape[1] // sp)
+    size = wide // 2
+    L = 64
+    count = sp * rows
+    nblocks = count // L
+
+    lane = lax.broadcasted_iota(jnp.int32, (go_ref.shape[0], wide), 1)
+    pairs = ((go_ref, gi_ref), (cv_ref, rw_ref), (kw_ref, vw_ref))
+    for p, (first, second) in enumerate(pairs):
+        for t in range(sp // 2):
+            x = first[:, t * wide : (t + 1) * wide].astype(jnp.float32)
+            y = second[:, t * wide : (t + 1) * wide].astype(jnp.float32)
+            cols = pl.ds(p * wide, wide)
+            even = jnp.where(lane < size, x, pltpu.roll(y, size, 1))
+            odd = jnp.where(lane < size, pltpu.roll(x, size, 1), y)
+            w_ref[2 * t, :, cols] = even.astype(jnp.bfloat16)
+            w_ref[2 * t + 1, :, cols] = odd.astype(jnp.bfloat16)
+    for t in range(sp):
+        o_ref[2 * t * size : (2 * t + 1) * size, :] = oc_ref[t * size : (t + 1) * size, :]
+        o_ref[(2 * t + 1) * size : (2 * t + 2) * size, :] = os_ref[t * size : (t + 1) * size, :]
+    mixed_ref[0:8, :] = jnp.zeros((8, size), jnp.float32)
+
+    line = [(lax.rem(z + d, sp), f, lax.rem(c + e, tp)) for d in range(sp) for e in range(tp)]
+    greet(line[1:] + fdev[1:])
+
+    def tok_at(zi, ci):
+        return toks.at[pl.ds(pl.multiple_of(zi * rows, rows), rows),
+                       pl.ds(pl.multiple_of(ci * feats, feats), feats)]
+
+    def out_at(zi, fi, ci):
+        return outs.at[pl.ds(pl.multiple_of(ci * orows, orows), orows),
+                       pl.ds(pl.multiple_of((zi * fs + fi) * ocols, ocols), ocols)]
+
+    local = [
+        pltpu.make_async_copy(w_ref.at[z], weights.at[z, f], loc_sem.at[0]),
+        pltpu.make_async_copy(tok_ref, tok_at(z, c), loc_sem.at[1]),
+        pltpu.make_async_copy(shift_ref.at[z], shifts.at[z], loc_sem.at[2]),
+        pltpu.make_async_copy(o_ref, out_at(z, f, c), loc_sem.at[3]),
+    ]
+    w_z = [send(w_ref.at[across[d]], weights.at[z, f], zs.at[d], zr.at[d], zdev[d])
+           for d in range(1, sp)]
+    s_z = [send(shift_ref.at[across[d]], shifts.at[z], hs.at[d], hr.at[d], zdev[d])
+           for d in range(1, sp)]
+    w_f = [[send(w_ref.at[z], weights.at[z, f], fs_s.at[0, e], fs_r.at[0, e], fdev[e])
+            for e in range(1, fs)]]
+    t_p = [send(tok_ref, tok_at(z, c), ps.at[0], pr.at[0], partner)]
+    t_z = [send(tok_ref, tok_at(z, c), ts.at[d], tr.at[d], zdev[d]) for d in range(1, sp)]
+    o_z = [send(o_ref, out_at(z, f, c), ozs.at[d], ozr.at[d], zdev[d]) for d in range(1, sp)]
+    for copy in local:
+        copy.start()
+    for d in range(1, sp):
+        w_z[d - 1].wait_recv()
+        got = weights.at[behind[d], f]
+        w_f.append([send(got, got, fs_s.at[d, e], fs_r.at[d, e], fdev[e]) for e in range(1, fs)])
+    o_f = [send(o_ref, out_at(z, f, c), ofs.at[0, e], ofr.at[0, e], fdev[e])
+           for e in range(1, fs)]
+    o_p = [send(o_ref, out_at(z, f, c), ops.at[0, 0], opr.at[0, 0], partner)]
+    for d in range(1, sp):
+        t_z[d - 1].wait_recv()
+        got = tok_at(behind[d], c)
+        t_p.append(send(got, got, ps.at[d], pr.at[d], partner))
+    for copy in local:
+        copy.wait()
+    for copies in w_f:
+        for copy in copies:
+            copy.wait_recv()
+
+    def pass_out(d):
+        o_z[d - 1].wait_recv()
+        got = out_at(behind[d], f, c)
+        o_p.append(send(got, got, ops.at[d, 0], opr.at[d, 0], partner))
+        o_f.extend(send(got, got, ofs.at[d, e], ofr.at[d, e], fdev[e]) for e in range(1, fs))
+
+    all_w = weights[...].reshape(sp * fs * w_ref.shape[1], w_ref.shape[2])
+    for d in range(sp):
+        t_p[d].wait_recv()
+        if d:
+            s_z[d - 1].wait_recv()
+        start = pl.multiple_of(behind[d] * rows, rows)
+        here = pl.ds(start, rows)
+        x = toks[here, :].astype(jnp.float32)
+        normed = (
+            x * lax.rsqrt(jnp.mean(x * x, axis=-1, keepdims=True) + RMS_EPS) * norm_ref[...]
+        ).astype(jnp.bfloat16)
+        proj = jnp.dot(normed, all_w, preferred_element_type=jnp.float32)
+        proj = proj.astype(jnp.bfloat16).astype(jnp.float32)
+        lows = jnp.dot(normed, low_ref[...], preferred_element_type=jnp.float32)
+        low_lane = lax.broadcasted_iota(jnp.int32, lows.shape, 1)
+        lows = jnp.where(low_lane < lows.shape[1] // 2, jnp.tanh(lows), lows)
+        pre = base_ref[...] + jnp.dot(
+            lows.astype(jnp.bfloat16), up_ref[...], preferred_element_type=jnp.float32
+        )
+        decay_sig, rate = halves(sigmoid(pre))
+        gate_out, gate_in = halves(proj[:, :wide])
+        conv_in, recv = halves(proj[:, wide : 2 * wide])
+        keys, vals = halves(proj[:, 2 * wide :])
+        column = jnp.transpose(shifts[behind[d]])[:, 0:1]
+        ld_ref[here, :] = -decay_sig * jnp.exp(column - 0.5)
+        unit = keys * lax.rsqrt(jnp.sum(keys * keys, axis=-1, keepdims=True) + UNIT_EPS)
+        a_ref[here, :] = -unit
+        b_ref[here, :] = unit * rate
+        k_ref[here, :] = keys * rate
+        r_ref[here, :] = recv
+        v_ref[here, :] = vals
+        gate_ref[here, :] = gate_out
+        mixed_ref[pl.ds(pl.multiple_of(start + 8, 8), rows), :] = gate_in * conv_in
+
+    fields = (ld_ref, a_ref, b_ref, k_ref, r_ref, v_ref)
+    bufs = (t_buf, g_buf, q_buf, o_buf)
+    group = 2
+    trips = nblocks // group
+    cuts = [trips * i // sp for i in range(sp + 1)]
+    for i in range(sp):
+        def several(n, _):
+            blocks_of(n * group, group, L, fields, sel_ref, bufs)
+            return 0
+
+        lax.fori_loop(cuts[i], cuts[i + 1], several, 0)
+        if i:
+            pass_out(i)
+
+    me = z * tp + c
+    mine = got_ref.at[:, pl.ds(pl.multiple_of((c * sp + z) * wide, wide), wide)]
+
+    def act_copy(n):
+        return pltpu.make_async_remote_copy(
+            src_ref=act_ref.at[n], dst_ref=mine, send_sem=act_s.at[n], recv_sem=act_r.at[me],
+            device_id=(n // tp, f, n % tp), device_id_type=MESH,
+        )
+
+    def own_copy(n):
+        return pltpu.make_async_copy(act_ref.at[n], mine, act_s.at[n])
+
+    def give(n):
+        @pl.when(me != n)
+        def _():
+            act_copy(n).start()
+
+        @pl.when(me == n)
+        def _():
+            own_copy(n).start()
+
+    state = jnp.zeros((size, size), jnp.float32)
+    taps = taps_ref[...]
+    for n in range(nblocks):
+        read = mm(q_buf[n], state) + o_buf[n]
+        state = mm(t_buf[n], state) + g_buf[n]
+        centred = read - jnp.mean(read, axis=-1, keepdims=True)
+        variance = jnp.mean(centred * centred, axis=-1, keepdims=True)
+        done = centred * lax.rsqrt(variance + GROUP_EPS) * gain_ref[...]
+        spot = n * L + 8
+        convolved = (
+            mixed_ref[spot - 2 : spot - 2 + L, :] * taps[0:1]
+            + mixed_ref[spot - 1 : spot - 1 + L, :] * taps[1:2]
+            + mixed_ref[spot : spot + L, :] * taps[2:3]
+        )
+        conv = gate_ref[n * L : (n + 1) * L, :] * convolved
+        act_ref[n] = jnp.concatenate([conv, done], axis=1).astype(jnp.bfloat16)
+        if n:
+            give(n - 1)
+    for d in range(sp):
+        for e in range(1, fs):
+            o_f[d * (fs - 1) + e - 1].wait_recv()
+            got = out_at(behind[d], lax.rem(f + fs - e, fs), c)
+            o_p.append(send(got, got, ops.at[d, e], opr.at[d, e], partner))
+        if d == 0:
+            give(nblocks - 1)
+    for n in range(nblocks):
+        @pl.when(me != n)
+        def _():
+            act_copy(n).wait_send()
+            pltpu.make_async_remote_copy(
+                src_ref=act_ref.at[n],
+                dst_ref=got_ref.at[:, pl.ds(((n % tp) * sp + n // tp) * wide, wide)],
+                send_sem=act_s.at[n], recv_sem=act_r.at[n],
+                device_id=partner, device_id_type=MESH,
+            ).wait_recv()
+
+        @pl.when(me == n)
+        def _():
+            own_copy(n).wait()
+    for copy in o_p:
+        copy.wait()
+    step = 512
+
+    def columns(i, _):
+        cols = pl.ds(pl.multiple_of(i * step, step), step)
+        out_ref[:, cols] = jnp.dot(
+            got_ref[...], outs[:, cols], preferred_element_type=jnp.float32
+        ).astype(out_ref.dtype)
+        return 0
+
+    lax.fori_loop(0, outs.shape[1] // step, columns, 0)
+    for copy in w_z + t_z + o_z + o_f + s_z:
+        copy.wait_send()
+    for copies in w_f:
+        for copy in copies:
+            copy.wait_send()
+    for copy in t_p:
+        copy.wait_send()
+
+
+def head_body(
+    tokens, norm_gain, conv_gate_out, conv_gate_in, conv_value, conv_taps, recv_weight,
+    key_weight, value_weight, decay_base, decay_down, decay_up, decay_shift, rate_base,
+    rate_down, rate_up, head_gain, out_conv, out_state,
+):
+    sp, fs, tp = (lax.axis_size(name) for name in ("sp", "fs", "tp"))
+    z = lax.axis_index("sp")
+    rows = tokens.shape[1]
+    size = recv_weight.shape[1] // sp
+    own_rows = conv_gate_out.shape[0]
+    tok = tokens.reshape(rows, tokens.shape[2])
+    shift = jnp.pad(decay_shift.reshape(rows, sp).T.reshape(sp, 1, rows), ((0, 0), (0, 7), (0, 0)))
+    low_w = jnp.concatenate([decay_down, rate_down], axis=1)
+
+    def mine(array):
+        return lax.dynamic_slice_in_dim(array, z * size, size, axis=array.ndim - 1)
+
+    up_d, up_r = mine(decay_up), mine(rate_up)
+    up = jnp.concatenate(
+        [jnp.concatenate([up_d, jnp.zeros_like(up_r)], axis=1),
+         jnp.concatenate([jnp.zeros_like(up_d), up_r], axis=1)], axis=0)
+    base = jnp.concatenate([mine(decay_base), mine(rate_base)]).reshape(1, 2 * size)
+    length = 64
+    count = sp * rows
+    nblocks = count // length
+    sel = jnp.asarray(range_rows(length), jnp.bfloat16)
+    vm = pl.BlockSpec(memory_space=pltpu.VMEM)
+    dma = pltpu.SemaphoreType.DMA
+    o_rows, o_cols = 2 * out_conv.shape[0], out_conv.shape[1]
+    model = out_conv.shape[1] * sp * fs
+    f32, bf16 = jnp.float32, jnp.bfloat16
+    field = pltpu.VMEM((count, size), f32)
+    block = pltpu.VMEM((nblocks, length, size), f32)
+    mixed = pl.pallas_call(
+        layer_kernel,
+        out_shape=jax.ShapeDtypeStruct((count // (sp * tp), model), bf16),
+        in_specs=[vm] * 17,
+        out_specs=vm,
+        scratch_shapes=[
+            pltpu.VMEM((count, tp * tok.shape[1]), bf16),
+            pltpu.VMEM((sp, own_rows, 6 * size), bf16),
+            pltpu.VMEM((sp, fs, own_rows, 6 * size), bf16),
+            pltpu.VMEM((o_rows, o_cols), bf16),
+            pltpu.VMEM((tp * o_rows, model), bf16),
+            pltpu.VMEM(shift.shape, f32),
+            field, field, field, field, field, field, field,
+            pltpu.VMEM((count + 8, size), f32),
+            block, block, block, block,
+            pltpu.VMEM((nblocks, length, 2 * size), bf16),
+            pltpu.VMEM((length, tp * o_rows), bf16),
+            dma((4,)), dma((sp,)), dma((sp,)), dma((sp, fs)), dma((sp, fs)), dma((sp,)), dma((sp,)),
+            dma((sp,)), dma((sp,)), dma((sp,)), dma((sp,)), dma((sp,)), dma((sp,)),
+            dma((sp, fs)), dma((sp, fs)), dma((sp, fs)), dma((sp, fs)),
+            dma((nblocks,)), dma((nblocks,)),
+        ],
+        compiler_params=pltpu.CompilerParams(
+            collective_id=0, has_side_effects=True, vmem_limit_bytes=56 * 1024 * 1024
+        ),
+    )(
+        tok, conv_gate_out, conv_gate_in, conv_value, recv_weight, key_weight, value_weight,
+        out_conv, out_state, shift, norm_gain.reshape(1, -1), low_w, up, base,
+        mine(conv_taps), mine(head_gain).reshape(1, size), sel,
+    )
+    return mixed.reshape((1,) + mixed.shape)
+
+
+def one_head_each(mesh, tokens, shift, weight):
+    sp, tp = mesh.shape["sp"], mesh.shape["tp"]
+    heads = shift.shape[2]
+    count = tokens.shape[1] // sp
+    size = weight.shape[1] // heads
+    return (
+        tp == 2
+        and heads == sp * tp
+        and tokens.shape[0] == mesh.shape["fs"]
+        and size == 64
+        and count == tp * 64
+        and sp % 2 == 0
+        and weight.shape[0] % (sp * mesh.shape["fs"] * 16) == 0
+    )
+
 
 def solution(mesh):
     placed = (
@@ -275,6 +713,11 @@
         P("tp", ("sp", "fs")),
         P("tp", ("sp", "fs")),
     )
-    return jax.shard_map(
-        body, mesh=mesh, in_specs=placed, out_specs=P("fs", ("sp", "tp"), None), check_vma=False
-    )
+    def run(*args):
+        chosen = head_body if one_head_each(mesh, args[0], args[12], args[6]) else body
+        return jax.shard_map(
+            chosen, mesh=mesh, in_specs=placed, out_specs=P("fs", ("sp", "tp"), None),
+            check_vma=False,
+        )(*args)
+
+    return run

time: 279 us -> 86.8 us (0.31)
  blocking collectives: 102 us -> 0 us
  matrix products: 85.6 us -> 0 us
  Pallas kernels: 0 us -> 77.4 us
  other arithmetic: 41.1 us -> 2.41 us
  waiting for transfers between devices: 28.4 us -> 0 us
  between operations: 13.7 us -> 0.06 us
  local copies, waits for them, and re-layouts: 3.01 us -> 6.72 us
    all_gather x11 -> x0, blocking collectives: 102 us -> none  [the longest x2 24.7 us: carried_in(): lax.all_gather(part.astype(kind), axis)]
    dot_general x58 -> x0, matrix products: 84.5 us -> none  [the longest x4 15.4 us: block_step(): jnp.einsum('htc,htsc,hsc->hts', remove_dir, damp_prior, key_rate, precisi...]
    pallas_call x0 -> x1, Pallas kernels: none -> 77.4 us  [head_body(): pl.pallas_call(layer_kernel, out_shape=jax.ShapeDtypeStruct((count // (sp...]
    another operation x24 -> x0, other arithmetic: 40.1 us -> none  [the longest x20 39.8 us: block_step(): lax.linalg.triangular_solve(unit_matrix - link_ab, rhs_terms, left_side=T...]
    reduce_scatter x1 -> x0, waiting for transfers between devices: 15.4 us -> none  [body(): lax.psum_scatter((jnp.dot(conv_out, conv_cols, preferred_element_type=jnp...]
    all_gather x8 -> x0, waiting for transfers between devices: 11.8 us -> none  [the longest x1 11.7 us: body(): lax.all_gather(local_vw, 'sp', axis=0, tiled=True)]
    unnamed x34 -> x19, local copies, waits for them, and re-layouts: 0.16 us -> 4.6 us
  transfers between devices with their start and end apart: 10 -> 0, of which waited for: 3 -> 0; matrix products, arithmetic and copies ran while one was open for 46% -> 0% of each run, Pallas kernels for 0% -> 0%
where the time goes in v2:
time: 86.8 us; the launch traced here: 86.6 us
  Pallas kernels  77.4 us (89%)
  local copies, waits for them, and re-layouts  6.72 us (8%)
  other arithmetic  2.41 us (3%)
    pallas_call x1, Pallas kernels, head_body(): pl.pallas_call(layer_kernel, out_shape=jax.ShapeDtypeStruct((count // (sp...  77.4 us
    unnamed x19, local copies, waits for them, and re-layouts  4.6 us

profile of v2, /device:TPU:11, one launch (start us, length us, event | category | flops | bytes accessed | tf_op | source)
XLA Modules:
  0.0 86.6 jit_solution(4436604551225748774)
XLA Ops:
  0.0 0.0 copy-start
  0.0 0.0 copy-start.4
  0.0 0.7 copy-done.4
  0.7 0.6 pad.6.shift_ref
  1.3 0.0 copy-start.1
  1.3 1.3 %copy.22 = bf16[2048,64]{1,0:T(8,128)(2,1)S(1)} copy(bf16[2048,64]{0,1:T(8,128)(2,1)} %param.34) | data formatting | bytes 524288 | tf_op args[14]
  2.6 0.0 copy-done.1
  2.6 0.3 copy.21
  2.9 0.0 copy-start.2
  2.9 0.0 copy-start.3
  2.9 1.1 %pad_maximum_fusion.low_ref = bf16[2048,128]{1,0:T(8,128)(2,1)} fusion(bf16[2048,64]{1,0:T(8,128)(2,1)S(1)} %copy.22, bf16[2048,64]{1,0:T(8,128)(2,1)S(1)} %copy.21), kind=kLoop, calls=%fused_computation | loop fusion | flops 1048576 | bytes 1048576 | tf_op jit(solution)/shard_map/concatenate | solution.py:624
  4.0 0.0 copy-done.2
  4.0 0.0 copy-done.3
  4.0 0.1 constant_dynamic-slice_fusion.1
  4.1 0.0 copy-start.5
  4.1 0.7 fusion.2.up_ref
  4.8 0.0 copy-done.5
  4.8 0.0 copy-start.6
  4.8 0.1 dynamic_slice.21
  4.9 0.6 copy-done.6
  5.5 0.1 dynamic_slice.20
  5.6 0.6 maximum_bitcast_fusion.base_ref
  6.2 0.0 copy-done
  6.2 0.0 copy-start.7
  6.2 0.6 constant_dynamic-slice_fusion.taps_ref
  6.8 0.0 copy-done.7
  6.9 0.6 dynamic-slice_bitcast_fusion.gain_ref
  7.5 77.4 %shard_map.190 = bf16[64,2048]{1,0:T(8,128)(2,1)} custom-call(bf16[128,1024]{1,0:T(8,128)(2,1)} %bitcast.13, bf16[128,256]{1,0:T(8,128)(2,1)} %go_ref.1, bf16[128,256]{1,0:T(8,128)(2,1)} %gi_ref.1, bf16[128,256]{1,0:T(8,128)(2,1)} %cv_ref.1, bf16[128,256]{1,0:T(8,128)(2,1)} %rw_ref.1, bf16[128,256]{1,0:T(8,128)(2,1)} %kw_ref.1, bf16[128,256]{1,0:T(8,128)(2,1)} %vw_ref.1, ...), custom_call_target="tpu_custom_call" | custom-call | tf_op jit(solution)/shard_map/pallas_call | solution.py:645
  84.9 1.7 %copy.24 = bf16[1,64,2048]{2,1,0:T(8,128)(2,1)} copy(bf16[1,64,2048]{2,1,0:T(8,128)(2,1)} %bitcast.12) | data formatting | bytes 524288
Async XLA Ops:
  0.0 6.2 %copy-start = (f32[3,256]{1,0:T(4,128)S(1)}, f32[3,256]{1,0:T(4,128)}, u32[]{:S(2)}) copy-start(f32[3,256]{1,0:T(4,128)} %param.25) | copy-start | bytes 9220
  0.0 0.7 copy-start.4
  1.3 1.3 %copy-start.1 = (bf16[2048,64]{0,1:T(8,128)(2,1)S(1)}, bf16[2048,64]{0,1:T(8,128)(2,1)}, u32[]{:S(2)}) copy-start(bf16[2048,64]{0,1:T(8,128)(2,1)} %param.30) | copy-start | bytes 786436
  2.9 1.1 %copy-start.2 = (bf16[64,256]{1,0:T(8,128)(2,1)S(1)}, bf16[64,256]{1,0:T(8,128)(2,1)}, u32[]{:S(2)}) copy-start(bf16[64,256]{1,0:T(8,128)(2,1)} %param.35) | copy-start | bytes 98308
  2.9 1.1 %copy-start.3 = (bf16[64,256]{1,0:T(8,128)(2,1)S(1)}, bf16[64,256]{1,0:T(8,128)(2,1)}, u32[]{:S(2)}) copy-start(bf16[64,256]{1,0:T(8,128)(2,1)} %param.31) | copy-start | bytes 98308
  4.1 0.7 copy-start.5
  4.8 0.7 copy-start.6
  6.2 0.7 copy-start.7

commit v3 on v2

--- a/solution.py
+++ b/solution.py
@@ -391,8 +391,9 @@
 
 def layer_kernel(
     tok_ref, go_ref, gi_ref, cv_ref, rw_ref, kw_ref, vw_ref, oc_ref, os_ref, shift_ref,
-    norm_ref, low_ref, up_ref, base_ref, taps_ref, gain_ref, sel_ref, out_ref,
-    toks, w_ref, weights, o_ref, outs, shifts, ld_ref, a_ref, b_ref, k_ref, r_ref, v_ref,
+    norm_ref, ddown_ref, rdown_ref, dup_ref, rup_ref, dbase_ref, rbase_ref, taps_ref, gain_ref,
+    sel_ref, out_ref,
+    toks, w_ref, weights, o_ref, outs, shift8_ref, shifts, ld_ref, a_ref, b_ref, k_ref, r_ref, v_ref,
     gate_ref, mixed_ref, t_buf, g_buf, q_buf, o_buf, act_ref, got_ref,
     loc_sem, zs, zr, fs_s, fs_r, ts, tr, ps, pr, hs, hr, ozs, ozr, ofs, ofr, ops, opr,
     act_s, act_r,
@@ -428,9 +429,23 @@
         o_ref[2 * t * size : (2 * t + 1) * size, :] = oc_ref[t * size : (t + 1) * size, :]
         o_ref[(2 * t + 1) * size : (2 * t + 2) * size, :] = os_ref[t * size : (t + 1) * size, :]
     mixed_ref[0:8, :] = jnp.zeros((8, size), jnp.float32)
+    for t in range(sp):
+        shift8_ref[t] = jnp.broadcast_to(shift_ref[t], shift8_ref.shape[1:])
 
     line = [(lax.rem(z + d, sp), f, lax.rem(c + e, tp)) for d in range(sp) for e in range(tp)]
     greet(line[1:] + fdev[1:])
+    pick = jnp.where(
+        lax.broadcasted_iota(jnp.int32, (sp * size, size), 0)
+        == z * size + lax.broadcasted_iota(jnp.int32, (sp * size, size), 1), 1.0, 0.0,
+    ).astype(jnp.float32)
+
+    def own_cols(ref):
+        return jnp.dot(ref[...], pick, precision=HIGHEST, preferred_element_type=jnp.float32)
+
+    def own_up(ref):
+        return jnp.dot(
+            ref[...], pick.astype(jnp.bfloat16), preferred_element_type=jnp.float32
+        ).astype(jnp.bfloat16)
 
     def tok_at(zi, ci):
         return toks.at[pl.ds(pl.multiple_of(zi * rows, rows), rows),
@@ -443,12 +458,12 @@
     local = [
         pltpu.make_async_copy(w_ref.at[z], weights.at[z, f], loc_sem.at[0]),
         pltpu.make_async_copy(tok_ref, tok_at(z, c), loc_sem.at[1]),
-        pltpu.make_async_copy(shift_ref.at[z], shifts.at[z], loc_sem.at[2]),
+        pltpu.make_async_copy(shift8_ref.at[z], shifts.at[z], loc_sem.at[2]),
         pltpu.make_async_copy(o_ref, out_at(z, f, c), loc_sem.at[3]),
     ]
     w_z = [send(w_ref.at[across[d]], weights.at[z, f], zs.at[d], zr.at[d], zdev[d])
            for d in range(1, sp)]
-    s_z = [send(shift_ref.at[across[d]], shifts.at[z], hs.at[d], hr.at[d], zdev[d])
+    s_z = [send(shift8_ref.at[across[d]], shifts.at[z], hs.at[d], hr.at[d], zdev[d])
            for d in range(1, sp)]
     w_f = [[send(w_ref.at[z], weights.at[z, f], fs_s.at[0, e], fs_r.at[0, e], fdev[e])
             for e in range(1, fs)]]
@@ -480,6 +495,10 @@
         o_p.append(send(got, got, ops.at[d, 0], opr.at[d, 0], partner))
         o_f.extend(send(got, got, ofs.at[d, e], ofr.at[d, e], fdev[e]) for e in range(1, fs))
 
+    dup, rup = own_up(dup_ref), own_up(rup_ref)
+    dbase, rbase, gain = own_cols(dbase_ref), own_cols(rbase_ref), own_cols(gain_ref)
+    taps = own_cols(taps_ref)
+    low_w = jnp.concatenate([ddown_ref[...], rdown_ref[...]], axis=0)
     all_w = weights[...].reshape(sp * fs * w_ref.shape[1], w_ref.shape[2])
     for d in range(sp):
         t_p[d].wait_recv()
@@ -493,13 +512,16 @@
         ).astype(jnp.bfloat16)
         proj = jnp.dot(normed, all_w, preferred_element_type=jnp.float32)
         proj = proj.astype(jnp.bfloat16).astype(jnp.float32)
-        lows = jnp.dot(normed, low_ref[...], preferred_element_type=jnp.float32)
-        low_lane = lax.broadcasted_iota(jnp.int32, lows.shape, 1)
-        lows = jnp.where(low_lane < lows.shape[1] // 2, jnp.tanh(lows), lows)
-        pre = base_ref[...] + jnp.dot(
-            lows.astype(jnp.bfloat16), up_ref[...], preferred_element_type=jnp.float32
+        lows = lax.dot_general(
+            normed, low_w, (((1,), (1,)), ((), ())), preferred_element_type=jnp.float32
         )
-        decay_sig, rate = halves(sigmoid(pre))
+        decay_low, rate_low = halves(lows)
+        decay_sig = sigmoid(dbase + jnp.dot(
+            jnp.tanh(decay_low).astype(jnp.bfloat16), dup, preferred_element_type=jnp.float32
+        ))
+        rate = sigmoid(rbase + jnp.dot(
+            rate_low.astype(jnp.bfloat16), rup, preferred_element_type=jnp.float32
+        ))
         gate_out, gate_in = halves(proj[:, :wide])
         conv_in, recv = halves(proj[:, wide : 2 * wide])
         keys, vals = halves(proj[:, 2 * wide :])
@@ -550,13 +572,12 @@
             own_copy(n).start()
 
     state = jnp.zeros((size, size), jnp.float32)
-    taps = taps_ref[...]
     for n in range(nblocks):
         read = mm(q_buf[n], state) + o_buf[n]
         state = mm(t_buf[n], state) + g_buf[n]
         centred = read - jnp.mean(read, axis=-1, keepdims=True)
         variance = jnp.mean(centred * centred, axis=-1, keepdims=True)
-        done = centred * lax.rsqrt(variance + GROUP_EPS) * gain_ref[...]
+        done = centred * lax.rsqrt(variance + GROUP_EPS) * gain
         spot = n * L + 8
         convolved = (
             mixed_ref[spot - 2 : spot - 2 + L, :] * taps[0:1]
@@ -615,22 +636,11 @@
     rate_down, rate_up, head_gain, out_conv, out_state,
 ):
     sp, fs, tp = (lax.axis_size(name) for name in ("sp", "fs", "tp"))
-    z = lax.axis_index("sp")
     rows = tokens.shape[1]
     size = recv_weight.shape[1] // sp
     own_rows = conv_gate_out.shape[0]
     tok = tokens.reshape(rows, tokens.shape[2])
-    shift = jnp.pad(decay_shift.reshape(rows, sp).T.reshape(sp, 1, rows), ((0, 0), (0, 7), (0, 0)))
-    low_w = jnp.concatenate([decay_down, rate_down], axis=1)
-
-    def mine(array):
-        return lax.dynamic_slice_in_dim(array, z * size, size, axis=array.ndim - 1)
-
-    up_d, up_r = mine(decay_up), mine(rate_up)
-    up = jnp.concatenate(
-        [jnp.concatenate([up_d, jnp.zeros_like(up_r)], axis=1),
-         jnp.concatenate([jnp.zeros_like(up_d), up_r], axis=1)], axis=0)
-    base = jnp.concatenate([mine(decay_base), mine(rate_base)]).reshape(1, 2 * size)
+    shift = decay_shift.reshape(rows, sp).T.reshape(sp, 1, rows)
     length = 64
     count = sp * rows
     nblocks = count // length
@@ -645,7 +655,7 @@
     mixed = pl.pallas_call(
         layer_kernel,
         out_shape=jax.ShapeDtypeStruct((count // (sp * tp), model), bf16),
-        in_specs=[vm] * 17,
+        in_specs=[vm] * 20,
         out_specs=vm,
         scratch_shapes=[
             pltpu.VMEM((count, tp * tok.shape[1]), bf16),
@@ -653,7 +663,8 @@
             pltpu.VMEM((sp, fs, own_rows, 6 * size), bf16),
             pltpu.VMEM((o_rows, o_cols), bf16),
             pltpu.VMEM((tp * o_rows, model), bf16),
-            pltpu.VMEM(shift.shape, f32),
+            pltpu.VMEM((sp, 8, rows), f32),
+            pltpu.VMEM((sp, 8, rows), f32),
             field, field, field, field, field, field, field,
             pltpu.VMEM((count + 8, size), f32),
             block, block, block, block,
@@ -669,8 +680,9 @@
         ),
     )(
         tok, conv_gate_out, conv_gate_in, conv_value, recv_weight, key_weight, value_weight,
-        out_conv, out_state, shift, norm_gain.reshape(1, -1), low_w, up, base,
-        mine(conv_taps), mine(head_gain).reshape(1, size), sel,
+        out_conv, out_state, shift, norm_gain.reshape(1, -1), decay_down.T, rate_down.T, decay_up,
+        rate_up, decay_base.reshape(1, -1), rate_base.reshape(1, -1), conv_taps,
+        head_gain.reshape(1, -1), sel,
     )
     return mixed.reshape((1,) + mixed.shape)
 

time: 86.8 us -> 80.5 us (0.927)
  local copies, waits for them, and re-layouts: 6.72 us -> 1.67 us
  other arithmetic: 2.41 us -> 0 us
  Pallas kernels: 77.4 us -> 78.6 us
    unnamed x19 -> x1, local copies, waits for them, and re-layouts: 4.6 us -> 1.67 us
    concatenate x2 -> x0, other arithmetic: 1.79 us -> none  [the longest x1 1.09 us: head_body(): low_w = jnp.concatenate([decay_down, rate_down], axis=1)]
    pallas_call x1, Pallas kernels: 77.4 us -> 78.6 us  [head_body(): pl.pallas_call(layer_kernel, out_shape=jax.ShapeDtypeStruct((count // (sp...]
    dynamic_slice x4 -> x0, local copies, waits for them, and re-layouts: 0.87 us -> none  [mine(): return lax.dynamic_slice_in_dim(array, z * size, size, axis=array.ndim - 1)]
where the time goes in v3:
time: 80.5 us; the launch traced here: 80.3 us
  Pallas kernels  78.6 us (98%)
  local copies, waits for them, and re-layouts  1.67 us (2%)
    pallas_call x1, Pallas kernels, head_body(): pl.pallas_call(layer_kernel, out_shape=jax.ShapeDtypeStruct((count // (sp...  78.6 us
    unnamed x1, local copies, waits for them, and re-layouts  1.67 us

profile of v3, /device:TPU:11, one launch (start us, length us, event | category | flops | bytes accessed | tf_op | source)
XLA Modules:
  0.0 80.3 jit_solution(8973811649768883524)
XLA Ops:
  0.0 78.6 %shard_map.190 = bf16[64,2048]{1,0:T(8,128)(2,1)} custom-call(bf16[128,1024]{1,0:T(8,128)(2,1)} %bitcast.14, bf16[128,256]{1,0:T(8,128)(2,1)} %go_ref.1, bf16[128,256]{1,0:T(8,128)(2,1)} %gi_ref.1, bf16[128,256]{1,0:T(8,128)(2,1)} %cv_ref.1, bf16[128,256]{1,0:T(8,128)(2,1)} %rw_ref.1, bf16[128,256]{1,0:T(8,128)(2,1)} %kw_ref.1, bf16[128,256]{1,0:T(8,128)(2,1)} %vw_ref.1, ...), custom_call_target="tpu_custom_call" | custom-call | tf_op jit(solution)/shard_map/pallas_call | solution.py:655
  78.6 1.7 %copy.22 = bf16[1,64,2048]{2,1,0:T(8,128)(2,1)} copy(bf16[1,64,2048]{2,1,0:T(8,128)(2,1)} %bitcast.13) | data formatting | bytes 524288
